TPU v7x, 256 devices: a whole 4x4x8 slice. The times are simulated.
256 devices in a mesh: sp: 64 (over z, y, core), tp: 4 (over x).
Axes of the slice: x: 4, y: 4, z: 8, core: 2. Of those that a mesh axis runs over, the one named last changes fastest.
Arguments:
- residual: bfloat16 [8192, 2048], P(('sp', 'tp')), may hold values from -6 to 6
- query_content: bfloat16 [8192, 1024], P('sp', 'tp'), may hold values from -400 to 400
- query_rotary: bfloat16 [8192, 384], P('sp', 'tp'), may hold values from -16 to 16
- key_latent: bfloat16 [8192, 512], P('sp'), may hold values from -6 to 6
- rotary_key: bfloat16 [8192, 32], P('sp'), may hold values from -6 to 6
- latent_gain: float32 [512], replicated, may hold values from 0.1 to 1.9
- key_weight: bfloat16 [512, 1024], P(None, 'tp'), may hold values from -0.25 to 0.25
- value_weight: bfloat16 [512, 1024], P(None, 'tp'), may hold values from -0.25 to 0.25
- output_gain: float32 [1024], P('tp'), may hold values from 0.1 to 1.9
- output_weight: bfloat16 [1024, 2048], P('tp'), may hold values from -0.1875 to 0.1875
- mixer_gain: float32 [2048], replicated, may hold values from 0.1 to 1.9
- gate_weight: bfloat16 [2048, 5632], P('sp', 'tp'), may hold values from -0.125 to 0.125
- up_weight: bfloat16 [2048, 5632], P('sp', 'tp'), may hold values from -0.125 to 0.125
- down_weight: bfloat16 [5632, 2048], P('tp', 'sp'), may hold values from -0.078125 to 0.078125
Outputs:
- layer_out: bfloat16 [8192, 2048], P(('sp', 'tp'))
All inputs are finite; a program needn't handle non-finite values.
Results may differ from a plain program's by a relative error of at most 0.015.
Values may be sent and summed in bfloat16 or wider, within the bound.
A program may use at most 128 MiB of HBM per device.

v0:
```python
import jax
import jax.numpy as jnp
from jax import lax
from jax.sharding import PartitionSpec as P

NARROW_HEADS = 8
WIDE_HEADS = 4
NARROW_DIM = 64
WIDE_DIM = 128
ROT_DIM = 32


epsilon = 1e-06
rope_base = 500000.0


def turned_gather(arrays, axis, dims):
    turned = [jnp.moveaxis(a, dim, 0) for a, dim in zip(arrays, dims)]
    both = jnp.concatenate([t.reshape(len(t), -1) for t in turned], axis=1)
    filled, at, done = (lax.all_gather(both, axis, axis=0, tiled=True), 0, [])
    for t, dim in zip(turned, dims):
        piece = filled[:, at : at + t[0].size].reshape(-1, *t.shape[1:])
        done.append(jnp.moveaxis(piece, 0, dim))
        at += t[0].size
    return tuple(done)


def side_by_side(arrays, axis, dim, along):
    widths = [a.shape[along] for a in arrays]
    both = jnp.concatenate(arrays, axis=along)
    filled = lax.all_gather(both, axis, axis=dim, tiled=True)
    return tuple(jnp.split(filled, [sum(widths[:k]) for k in range(1, len(widths))], axis=along))


def split_up(x, dim, size):
    before, after = (x.shape[:dim], x.shape[dim + 1 :])
    return jnp.moveaxis(x.reshape(*before, size, -1, *after), dim, 0)


def summed_on_arrival(x, axis, dim):
    pieces = split_up(x, dim, lax.axis_size(axis))
    arrived = lax.all_to_all(pieces, axis, split_axis=0, concat_axis=0, tiled=True)
    return arrived.astype(jnp.float32).sum(axis=0)


def normalize(values):
    values = values.astype(jnp.float32)
    return values * lax.rsqrt(jnp.mean(values * values, axis=-1, keepdims=True) + epsilon)


def rotate(values, positions):
    half_width = values.shape[-1] // 2
    inverse = 1.0 / jnp.power(
        rope_base, jnp.arange(0, 2 * half_width, 2, dtype=jnp.float32) / (2 * half_width)
    )
    angles = positions.astype(jnp.float32)[:, None] * inverse[None, :]
    table_shape = (angles.shape[0],) + (1,) * (values.ndim - 2) + (half_width,)
    cosine_table = jnp.cos(angles).reshape(table_shape)
    sine_table = jnp.sin(angles).reshape(table_shape)
    first_half = values[..., :half_width]
    second_half = values[..., half_width:]
    return jnp.concatenate(
        [
            first_half * cosine_table - second_half * sine_table,
            second_half * cosine_table + first_half * sine_table,
        ],
        axis=-1,
    )


def group_update(carried, query_part, rotary_part, key_part, rotary_keys, value_part, factor):
    running_max, totals, accumulated = carried
    scores = (
        jnp.einsum("qhd,khd->hqk", query_part, key_part, preferred_element_type=jnp.float32)
        + jnp.einsum("qhd,kd->hqk", rotary_part, rotary_keys, preferred_element_type=jnp.float32)
    ) * factor
    new_max = jnp.max(scores, axis=-1)
    shrink = jnp.exp(running_max - new_max)
    powers = jnp.exp(scores - new_max[..., None])
    totals = totals * shrink + jnp.sum(powers, axis=-1)
    added = jnp.einsum(
        "hqk,khd->qhd", powers.astype(jnp.bfloat16), value_part, preferred_element_type=jnp.float32
    )
    accumulated = accumulated * jnp.transpose(shrink)[:, :, None] + added
    return (new_max, totals, accumulated)


def on_device(
    residual,
    query_content,
    query_rotary,
    key_latent,
    rotary_key,
    latent_gain,
    key_weight,
    value_weight,
    output_gain,
    output_weight,
    mixer_gain,
    gate_weight,
    up_weight,
    down_weight,
):
    tp_count = lax.axis_size("tp")
    narrow_dev = NARROW_HEADS // tp_count
    wide_dev = WIDE_HEADS // tp_count
    row_count = key_latent.shape[0]
    gate_whole, up_whole, down_whole = turned_gather(
        (gate_weight, up_weight, down_weight), "sp", (0, 0, 1)
    )
    positions = lax.axis_index("sp") * row_count + lax.iota(jnp.int32, row_count)
    latent = (normalize(key_latent) * latent_gain).astype(jnp.bfloat16)
    key_rows = jnp.dot(latent, key_weight, preferred_element_type=jnp.float32).astype(jnp.bfloat16)
    value_rows = jnp.dot(latent, value_weight, preferred_element_type=jnp.float32).astype(
        jnp.bfloat16
    )
    rot_keys = rotate(rotary_key.astype(jnp.float32), positions).astype(jnp.bfloat16)
    head_count = narrow_dev + wide_dev
    rot_queries = rotate(
        query_rotary.astype(jnp.float32).reshape(row_count, head_count, ROT_DIM), positions
    ).astype(jnp.bfloat16)
    narrow_cols = narrow_dev * NARROW_DIM
    query_narrow = query_content[:, :narrow_cols].reshape(row_count, narrow_dev, NARROW_DIM)
    query_wide = query_content[:, narrow_cols:].reshape(row_count, wide_dev, WIDE_DIM)
    rotary_narrow = rot_queries[:, :narrow_dev]
    rotary_wide = rot_queries[:, narrow_dev:]
    narrow_factor = (NARROW_DIM + ROT_DIM) ** (-0.5)
    wide_factor = (WIDE_DIM + ROT_DIM) ** (-0.5)

    def start_state(count, width):
        return (
            jnp.full((count, row_count), -jnp.inf, jnp.float32),
            jnp.zeros((count, row_count), jnp.float32),
            jnp.zeros((row_count, count, width), jnp.float32),
        )

    carried = (start_state(narrow_dev, NARROW_DIM), start_state(wide_dev, WIDE_DIM))
    piece_keys, piece_rotary, piece_values = side_by_side(
        (key_rows, rot_keys, value_rows), "sp", 0, 1
    )
    length = piece_keys.shape[0]
    narrow_keys = piece_keys[:, :narrow_cols].reshape(length, narrow_dev, NARROW_DIM)
    wide_keys = piece_keys[:, narrow_cols:].reshape(length, wide_dev, WIDE_DIM)
    narrow_values = piece_values[:, :narrow_cols].reshape(length, narrow_dev, NARROW_DIM)
    wide_values = piece_values[:, narrow_cols:].reshape(length, wide_dev, WIDE_DIM)
    narrow_state = group_update(
        carried[0],
        query_narrow,
        rotary_narrow,
        narrow_keys,
        piece_rotary,
        narrow_values,
        narrow_factor,
    )
    wide_state = group_update(
        carried[1], query_wide, rotary_wide, wide_keys, piece_rotary, wide_values, wide_factor
    )
    narrow_state, wide_state = (narrow_state, wide_state)

    def finish(carried):
        return normalize(carried[2] / jnp.transpose(carried[1])[:, :, None]).reshape(row_count, -1)

    mixed = (
        jnp.concatenate([finish(narrow_state), finish(wide_state)], axis=1) * output_gain
    ).astype(jnp.bfloat16)
    projected = summed_on_arrival(
        jnp.dot(mixed, output_weight, preferred_element_type=jnp.float32).astype(jnp.bfloat16),
        "tp",
        0,
    )
    middle = (residual.astype(jnp.float32) + projected).astype(jnp.bfloat16)
    normed = (normalize(middle) * mixer_gain).astype(jnp.bfloat16)
    block_normed = lax.all_gather(normed, "tp", axis=0, tiled=True)
    gate_sums = jnp.dot(block_normed, gate_whole, preferred_element_type=jnp.float32)
    up_sums = jnp.dot(block_normed, up_whole, preferred_element_type=jnp.float32)
    hidden = (jax.nn.silu(gate_sums) * up_sums).astype(jnp.bfloat16)
    channel_out = summed_on_arrival(
        jnp.dot(hidden, down_whole, preferred_element_type=jnp.float32).astype(jnp.bfloat16),
        "tp",
        0,
    )
    return (middle.astype(jnp.float32) + channel_out).astype(jnp.bfloat16)


def solution(mesh):
    placed = (
        P(("sp", "tp"), None),
        P("sp", "tp"),
        P("sp", "tp"),
        P("sp", None),
        P("sp", None),
        P(),
        P(None, "tp"),
        P(None, "tp"),
        P("tp"),
        P("tp", None),
        P(),
        P("sp", "tp"),
        P("sp", "tp"),
        P("tp", "sp"),
    )
    return jax.shard_map(
        on_device, mesh=mesh, in_specs=placed, out_specs=P(("sp", "tp"), None), check_vma=False
    )
```

profile of v0, /device:TPU:1, one launch (start us, length us, event | category | flops | bytes accessed | tf_op | source)
XLA Modules:
  0.0 234.1 jit_solution(12337247251630548791)
XLA Ops:
  6.5 0.0 copy-start
  6.5 0.0 all-gather.3.cloned.1.call-start
  6.6 0.8 convert_element_type.70
  7.3 0.1 multiply_cosine_fusion
  7.5 0.1 copy.31
  7.6 0.1 copy.32
  7.7 1.0 fusion.67
  8.8 1.3 convolution_convert_fusion.1
  10.0 1.3 convolution_convert_fusion.2
  11.3 0.8 pad_maximum_fusion.1
  12.1 0.0 all-gather.3.cloned.1.call-update
  12.1 0.0 all-gather.5.cloned.1.call-start
  12.2 1.7 pad_maximum_fusion
  13.9 0.0 all-gather.5.cloned.1.call-update
  13.9 0.7 convert.17
  14.7 0.8 slice.52
  15.4 0.1 copy.34
  15.6 86.9 %all-gather.3.cloned.1.call-done = bf16[8192,544]{1,0:T(8,128)(2,1)} async-done(((bf16[128,544]{1,0:T(8,128)(2,1)}), bf16[8192,544]{1,0:T(8,128)(2,1)}) %all-gather.3.cloned.1.call-update) | async-done | bytes 8912912 | tf_op jit(solution)/shard_map/all_gather | solution.py:31
  102.4 5.7 %fusion.90 = (bf16[8192,128]{1,0:T(8,128)(2,1)}, bf16[8192,128]{1,0:T(8,128)(2,1)}) fusion(bf16[8192,544]{1,0:T(8,128)(2,1)} %all-gather.3.cloned.1.call-done), kind=kLoop, calls=%fused_computation.99 | loop fusion | bytes 8388608 | tf_op jit(solution)/shard_map/slice | solution.py:142
  108.1 2.9 %copy.33 = bf16[8192,128]{0,1:T(8,128)(2,1)S(1)} copy(bf16[8192,128]{1,0:T(8,128)(2,1)} %get-tuple-element.7) | data formatting | bytes 4194304 | tf_op jit(solution)/shard_map/slice | solution.py:142
  111.0 4.1 %copy.36 = bf16[8192,128]{0,1:T(8,128)(2,1)} copy(bf16[8192,128]{1,0:T(8,128)(2,1)} %get-tuple-element.8) | data formatting | bytes 4194304 | tf_op jit(solution)/shard_map/slice | solution.py:144
  115.1 0.0 copy-start.3
  115.1 2.3 convolution_bitcast_fusion.2
  117.4 0.0 copy-done.3
  117.5 2.9 %fusion.91 = (f32[128]{0:T(128)S(1)}, f32[1,128,8192]{1,2,0:T(8,128)S(1)}) fusion(f32[1,128,8192]{1,2,0:T(8,128)S(1)} %convolution_bitcast_fusion.2, bf16[128,256]{1,0:T(8,128)(2,1)S(1)} %copy-done.3, bf16[8192,544]{1,0:T(8,128)(2,1)} %all-gather.3.cloned.1.call-done), kind=kOutput, calls=%fused_computation.100 | convolution fusion | flops 271581056 | bytes 10519040 | tf_op jit(solution)/shard_map/qhd,khd->hqk/dot_general | solution.py:74
  120.3 1.1 fusion.15
  121.4 3.9 %multiply_reduce_fusion = (f32[128]{0:T(128)S(1)}, f32[1,128,128]{2,1,0:T(8,128)S(1)}) fusion(f32[128]{0:T(128)S(1)} %get-tuple-element.18, f32[1,128,8192]{1,2,0:T(8,128)S(1)} %get-tuple-element.20, f32[128]{0:T(128)S(1)} %get-tuple-element.19, bf16[8192,544]{1,0:T(8,128)(2,1)} %all-gather.3.cloned.1.call-done, f32[128]{0:T(128)S(1)} %get-tuple-element.17), kind=kOutput, calls=%fused_computation.69 | convolution fusion | flops 270598016 | bytes 6359040 | tf_op jit(solution)/shard_map/hqk,khd->qhd/dot_general | solution.py:81
  125.3 2.8 %convolution_bitcast_fusion = f32[2,128,8192]{1,2,0:T(8,128)S(1)} fusion(bf16[8192,544]{1,0:T(8,128)(2,1)} %all-gather.3.cloned.1.call-done, bf16[128,3,16]{0,2,1:T(8,128)(2,1)S(1)} %get-tuple-element.9, bf16[128,3,16]{0,2,1:T(8,128)(2,1)S(1)} %get-tuple-element.10), kind=kOutput, calls=%fused_computation | convolution fusion | flops 134250496 | bytes 10510336 | tf_op jit(solution)/shard_map/qhd,kd->hqk/dot_general | solution.py:75
  128.2 2.1 fusion.92
  130.3 0.0 copy-start.1
  130.3 1.1 fusion.4
  131.5 0.5 copy-done.1
  131.9 0.0 copy-start.5
  131.9 0.0 copy-start.2
  131.9 1.6 multiply_reduce_fusion.1
  133.6 0.0 copy-start.4
  133.6 0.0 copy-done
  133.6 0.0 copy-done.5
  133.6 0.4 convolution_convert_fusion
  134.1 12.9 %all_to_all.10 = bf16[4,32,2048]{2,1,0:T(8,128)(2,1)S(1)} all-to-all(bf16[4,32,2048]{2,1,0:T(8,128)(2,1)S(1)} %bitcast.78), channel_id=1, replica_groups=mesh['sp'=64,'tp'=4] {'tp'}, dimensions={0} | all-to-all | bytes 1048576 | tf_op jit(solution)/shard_map/all_to_all | solution.py:42
  147.0 0.1 convert_reduce_fusion.1
  147.0 0.0 copy-done.2
  147.0 0.2 fusion.70
  147.2 0.0 copy-done.4
  147.2 0.1 fusion.72
  147.3 11.0 %all_gather.10 = bf16[128,2048]{1,0:T(8,128)(2,1)S(1)} all-gather(bf16[32,2048]{1,0:T(8,128)(2,1)S(1)} %fusion.72), channel_id=1, replica_groups=mesh['sp'=64,'tp'=4] {'tp'}, dimensions={0}, use_global_device_ids=true | all-gather | bytes 655360 | tf_op jit(solution)/shard_map/all_gather | solution.py:173
  158.3 44.5 %all-gather.5.cloned.1.call-done = bf16[2048,4224]{1,0:T(8,128)(2,1)} async-done(((bf16[32,4224]{1,0:T(8,128)(2,1)}), bf16[2048,4224]{1,0:T(8,128)(2,1)}) %all-gather.5.cloned.1.call-update) | async-done | bytes 17301520 | tf_op jit(solution)/shard_map/all_gather | solution.py:20
  202.8 3.6 %fusion.10 = f32[128,1408]{1,0:T(8,128)S(1)} fusion(bf16[128,2048]{1,0:T(8,128)(2,1)S(1)} %all_gather.10, bf16[2048,4224]{1,0:T(8,128)(2,1)} %all-gather.5.cloned.1.call-done), kind=kOutput, calls=%fused_computation.15 | convolution fusion | flops 738197504 | bytes 7012352 | tf_op jit(solution)/shard_map/dot_general | solution.py:174
  206.5 7.2 %fusion.20 = bf16[128,2048]{1,0:T(8,128)(2,1)S(1)} fusion(bf16[2048,4224]{1,0:T(8,128)(2,1)} %all-gather.5.cloned.1.call-done, bf16[128,2048]{1,0:T(8,128)(2,1)S(1)} %all_gather.10, f32[128,1408]{1,0:T(8,128)S(1)} %fusion.10), kind=kOutput, calls=%fused_computation.23 | convolution fusion | flops 1477738496 | bytes 13303808 | tf_op jit(solution)/shard_map/dot_general | solution.py:178
  213.7 12.8 %all_to_all.11 = bf16[4,32,2048]{2,1,0:T(8,128)(2,1)S(1)} all-to-all(bf16[4,32,2048]{2,1,0:T(8,128)(2,1)S(1)} %bitcast.79), channel_id=1, replica_groups=mesh['sp'=64,'tp'=4] {'tp'}, dimensions={0} | all-to-all | bytes 1048576 | tf_op jit(solution)/shard_map/all_to_all | solution.py:42
  226.5 0.1 convert_reduce_fusion
  226.6 0.7 fusion.73
  (12 shorter events, 0.1 us)
Async XLA Ops:
  6.5 127.1 %copy-start = (bf16[256,2048]{1,0:T(8,128)(2,1)S(1)}, bf16[256,2048]{1,0:T(8,128)(2,1)}, u32[]{:S(2)}) copy-start(bf16[256,2048]{1,0:T(8,128)(2,1)} %param.23) | copy-start | bytes 3145732
  6.5 95.9 %all-gather.3.cloned.1.call-start = ((), (), s32[]{:S(2)}) async-start(), calls=%async_computation.2 | async-start | bytes 10649600 | tf_op jit(solution)/shard_map/all_gather | solution.py:31
  12.1 190.7 %all-gather.5.cloned.1.call-start = ((), (), s32[]{:S(2)}) async-start(), calls=%async_computation.3 | async-start | bytes 17571840 | tf_op jit(solution)/shard_map/all_gather | solution.py:20
  115.1 2.3 copy-start.3
  130.3 1.6 copy-start.1
  131.9 1.7 copy-start.5
  131.9 15.1 %copy-start.2 = (bf16[32,2048]{1,0:T(8,128)(2,1)S(1)}, bf16[32,2048]{1,0:T(8,128)(2,1)}, u32[]{:S(2)}) copy-start(bf16[32,2048]{1,0:T(8,128)(2,1)} %param.14) | copy-start | bytes 393220
  133.6 13.6 %copy-start.4 = (f32[2048]{0:T(1024)S(1)}, f32[2048]{0:T(1024)}, u32[]{:S(2)}) copy-start(f32[2048]{0:T(1024)} %param.24) | copy-start | bytes 24580
Sparse Core Ops, SparseCore 0:
  12.2 90.1 all-gather.2
  105.2 97.6 all-gather.4
where the time goes:
time: 235 us; the launch traced here: 234 us
  waiting for transfers between devices  131 us (56%)
  blocking collectives  36.7 us (16%)
  matrix products  29.5 us (13%)
  local copies, waits for them, and re-layouts  14.3 us (6%)
  between operations  13.6 us (6%)
  other arithmetic  8.62 us (4%)
    all_gather x1, waiting for transfers between devices, side_by_side(): filled = lax.all_gather(both, axis, axis=dim, tiled=True)  86.9 us
    all_gather x1, waiting for transfers between devices, turned_gather(): filled, at, done = (lax.all_gather(both, axis, axis=0, tiled=True), 0, [])  44.5 us
    all_to_all x2, blocking collectives, summed_on_arrival(): lax.all_to_all(pieces, axis, split_axis=0, concat_axis=0, tiled=True)  25.7 us
    all_gather x1, blocking collectives, on_device(): block_normed = lax.all_gather(normed, 'tp', axis=0, tiled=True)  11 us
    slice x2, local copies, waits for them, and re-layouts, on_device(): piece_keys[:, :narrow_cols].reshape(length, narrow_dev, NARROW_DIM)  8.56 us
    dot_general x1, matrix products, on_device(): jnp.dot(hidden, down_whole, preferred_element_type=jnp.float32)  7.23 us
    dot_general x2, matrix products, group_update(): jnp.einsum('hqk,khd->qhd', powers.astype(jnp.bfloat16), value_part, prefe...  5.53 us
    dot_general x2, matrix products, group_update(): jnp.einsum('qhd,kd->hqk', rotary_part, rotary_keys, preferred_element_typ...  5.16 us
  transfers between devices with their start and end apart: 2, of which 2 were waited for; matrix products, arithmetic and copies ran while one was open for 15% of the time, Pallas kernels for 0%

commit v1 on v0

v1 whole, which is shorter than its diff:
```python
import functools

import jax
import jax.numpy as jnp
from jax import lax
from jax.experimental import pallas as pl
from jax.experimental.pallas import tpu as pltpu
from jax.sharding import PartitionSpec as P

NY = 4
ROT_DIM = 32
EPS = 1e-06
ROPE_BASE = 500000.0
LOG2E = 1.4426950408889634
MESH = pl.DeviceIdType.MESH
F32 = jnp.float32
BF16 = jnp.bfloat16


def dot(a, b):
    return lax.dot_general(a, b, (((1,), (0,)), ((), ())), preferred_element_type=F32)


def dot_nt(a, b):
    return lax.dot_general(a, b, (((1,), (1,)), ((), ())), preferred_element_type=F32)


def hops(n):
    both = list(range(1, (n - 1) // 2 + 1))
    return both, (n // 2 if n % 2 == 0 and n > 1 else None)


def kernel(
    NZ,
    NX,
    scales,
    cos_ref,
    sin_ref,
    qc_ref,
    qr_ref,
    lat_ref,
    rk_ref,
    lgain_ref,
    kw_ref,
    vw_ref,
    ogain_ref,
    mgain_ref,
    resid_hbm,
    ow_hbm,
    gate_hbm,
    up_hbm,
    down_hbm,
    out_ref,
    w,
    kv,
    qall,
    qx,
    acc,
    mrow,
    lrow,
    osend,
    orecv,
    ssend,
    srecv,
    mixed,
    wo,
    resid,
    mid,
    normed,
    accg,
    accu,
    hid,
    part,
    rsum,
    loc_sem,
    kv_s,
    kv_r,
    kvp_s,
    kvp_r,
    q_s,
    q_r,
    o_s,
    o_r,
    st_s,
    st_r,
    mx_s,
    mx_r,
    wo_s,
    wo_r,
    wop_s,
    wop_r,
    re_s,
    re_r,
    rs_s,
    rs_r,
    w_s1,
    w_s2,
    wp_s,
    w_r1,
    w_r2,
    wp_r,
):
    sp = lax.axis_index("sp")
    x = lax.axis_index("tp")
    c = sp % 2
    y = (sp // 2) % NY
    z = sp // (2 * NY)
    T = qc_ref.shape[0]
    R = resid.shape[1]
    D = resid.shape[2]
    pend = []

    def dev(zz=None, yy=None, cc=None, xx=None):
        zz = z if zz is None else (zz + 2 * NZ) % NZ
        yy = y if yy is None else (yy + 2 * NY) % NY
        cc = c if cc is None else cc
        xx = x if xx is None else (xx + 2 * NX) % NX
        return ((zz * NY + yy) * 2 + cc, xx)

    def send(src, dst, ssem, rsem, device, keep=True):
        d = pltpu.make_async_remote_copy(
            src_ref=src, dst_ref=dst, send_sem=ssem, recv_sem=rsem, device_id=device, device_id_type=MESH
        )
        d.start()
        if keep:
            pend.append(d)

    def arrived(ref, sem):
        pltpu.make_async_copy(ref, ref, sem).wait()

    def core0(f):
        pl.when(c == 0)(f)

    def core1(f):
        pl.when(c == 1)(f)

    partner = dev(cc=1 - c)
    dirc = 1 - 2 * c
    zboth, zlast = hops(NZ)
    yboth, ylast = hops(NY)
    xboth, xlast = hops(NX)

    loc = [
        pltpu.make_async_copy(resid_hbm, resid.at[x], loc_sem.at[0]),
        pltpu.make_async_copy(ow_hbm, wo.at[x], loc_sem.at[1]),
        pltpu.make_async_copy(gate_hbm, w.at[0, z, y, c], loc_sem.at[2]),
        pltpu.make_async_copy(up_hbm, w.at[1, z, y, c], loc_sem.at[3]),
        pltpu.make_async_copy(down_hbm, w.at[2, z, y, c], loc_sem.at[4]),
    ]
    for d in loc:
        d.start()

    barrier = pltpu.get_barrier_semaphore()
    peers = [partner]
    peers += [dev(zz=z + 1)] + ([dev(zz=z - 1)] if NZ > 2 else [])
    peers += [dev(yy=y + k) for k in range(1, NY)]
    peers += [dev(xx=x + k) for k in range(1, NX)]
    for p in peers:
        pl.semaphore_signal(barrier, inc=1, device_id=p, device_id_type=MESH)

    lane_q = lax.broadcasted_iota(jnp.int32, (qr_ref.shape[1], 128), 1)
    row_q = lax.broadcasted_iota(jnp.int32, (qr_ref.shape[1], 128), 0)
    half = ROT_DIM // 2
    swapped_q = jnp.where(lane_q % ROT_DIM < half, lane_q + half, lane_q - half)
    qr = qr_ref[...]
    q_same = dot(qr, (row_q == lane_q).astype(BF16))
    q_swap = dot(qr, (row_q == swapped_q).astype(BF16))
    cos = cos_ref[...]
    sin = sin_ref[...]
    qall[0, :, 0:128] = qc_ref[:, 0:128]
    qall[0, :, 128:256] = (q_same * cos + q_swap * sin).astype(BF16)
    qall[0, :, 256:384] = qc_ref[:, 128:256]

    lane_k = lax.broadcasted_iota(jnp.int32, (ROT_DIM, 128), 1)
    row_k = lax.broadcasted_iota(jnp.int32, (ROT_DIM, 128), 0)
    lane_in = lane_k % ROT_DIM
    swapped_k = jnp.where(lane_in < half, lane_in + half, lane_in - half)
    rk = rk_ref[...]
    k_same = dot(rk, (row_k == lane_in).astype(BF16))
    k_swap = dot(rk, (row_k == swapped_k).astype(BF16))
    lat = lat_ref[...].astype(F32)
    lat = lat * lax.rsqrt(jnp.mean(lat * lat, axis=-1, keepdims=True) + EPS)
    lat = (lat * lgain_ref[...]).astype(BF16)
    keys = dot(lat, kw_ref[...]).astype(BF16)
    vals = jnp.transpose(dot(lat, vw_ref[...])).astype(BF16)
    kv[0, c, :, 0:128] = keys[:, 0:128]
    kv[0, c, :, 128:256] = (k_same * cos + k_swap * sin).astype(BF16)
    kv[0, c, :, 256:384] = keys[:, 128:256]
    kv[0, c, :, 384:512] = vals[0:128, :]
    kv[0, c, :, 512:640] = vals[128:256, :]

    pl.semaphore_wait(barrier, len(peers))

    def kv_copy(src_slot, dst_slot, device):
        send(kv.at[src_slot, c], kv.at[dst_slot, c], kv_s.at[dst_slot], kv_r.at[dst_slot], device)

    def kv_partner(slot):
        send(kv.at[slot, c], kv.at[slot, c], kvp_s.at[slot], kvp_r.at[slot], partner)

    def kv_send(r):
        if r in zboth:
            kv_copy(2 * r - 3 if r > 1 else 0, 2 * r - 1, dev(zz=z + 1))
            kv_copy(2 * r - 2 if r > 1 else 0, 2 * r, dev(zz=z - 1))
        elif r == zlast:
            kv_copy((2 * r - 3 + c) if r > 1 else 0, NZ - 1, dev(zz=z + dirc))

    def slots_of(n, r):
        if r == 0:
            return [0]
        return [2 * r - 1, 2 * r] if r <= (n - 1) // 2 else [n - 1]

    def offset_of(n, slot):
        if slot == 0:
            return 0
        return slot_r(n, slot) if slot % 2 == 0 else -slot_r(n, slot)

    def slot_r(n, slot):
        return (slot + 1) // 2

    def zpos(slot):
        return (z + offset_of(NZ, slot) + 2 * NZ) % NZ

    def ypos(slot):
        return (y + offset_of(NY, slot) + 2 * NY) % NY

    kv_send(1)
    kv_partner(0)
    for k in range(1, NY):
        send(qall.at[0], qall.at[NY - k], q_s.at[k], q_r.at[NY - k], dev(yy=y + k))

    for d in loc:
        d.wait()

    def wo_send(r):
        if r in xboth:
            send(wo.at[(x - r + 1 + NX) % NX, c], wo.at[(x - r + 1 + NX) % NX, c], wo_s.at[2 * r - 1], wo_r.at[2 * r - 1], dev(xx=x + 1))
            send(wo.at[(x + r - 1) % NX, c], wo.at[(x + r - 1) % NX, c], wo_s.at[2 * r], wo_r.at[2 * r], dev(xx=x - 1))
        elif r == xlast:
            p = (x - dirc * (r - 1) + 2 * NX) % NX
            send(wo.at[p, c], wo.at[p, c], wo_s.at[NX - 1], wo_r.at[NX - 1], dev(xx=x + dirc))

    def wo_wait(r):
        for slot in slots_of(NX, r):
            p = (x + offset_of(NX, slot) + 2 * NX) % NX
            arrived(wo.at[p, c], wo_r.at[slot])
            send(wo.at[p, c], wo.at[p, c], wop_s.at[slot], wop_r.at[slot], partner)

    for k in range(1, NX):
        send(resid.at[x], resid.at[x], re_s.at[k], re_r.at[NX - k], dev(xx=x + k))
    if NX > 1:
        wo_send(1)

    def zdir(m):
        return dirc * (1 - 2 * (m % 2))

    def ring_y(m, zz, cc, r, ssem, rsems):
        if r in yboth:
            a, b = (y - r + 1 + NY) % NY, (y + r - 1) % NY
            send(w.at[m, zz, a, cc], w.at[m, zz, a, cc], ssem, rsems(2 * r - 1), dev(yy=y + 1), False)
            send(w.at[m, zz, b, cc], w.at[m, zz, b, cc], ssem, rsems(2 * r), dev(yy=y - 1), False)
        elif r == ylast:
            p = (y - zdir(m) * (r - 1) + 2 * NY) % NY
            send(w.at[m, zz, p, cc], w.at[m, zz, p, cc], ssem, rsems(NY - 1), dev(yy=y + zdir(m)), False)

    def ring_z(m, view, r, ssem, rsems):
        if r in zboth:
            a, b = (z - r + 1 + NZ) % NZ, (z + r - 1) % NZ
            send(view(a), view(a), ssem, rsems(2 * r - 1), dev(zz=z + 1), False)
            send(view(b), view(b), ssem, rsems(2 * r), dev(zz=z - 1), False)
        elif r == zlast:
            p = (z - zdir(m) * (r - 1) + 2 * NZ) % NZ
            send(view(p), view(p), ssem, rsems(NZ - 1), dev(zz=z + zdir(m)), False)

    def a1_send(m, r):
        ring_y(m, z, 0, r, w_s1.at[m], lambda s: w_r1.at[m, s])

    def a1_wait(m, r):
        for slot in slots_of(NY, r):
            arrived(w.at[m, z, ypos(slot), 0], w_r1.at[m, slot])

    def a_block(m, zz):
        return w.at[m, zz, :, 0]

    def a2_send(m, r):
        ring_z(m, lambda p: a_block(m, p), r, w_s2.at[m], lambda s: w_r2.at[m, s, 0])

    def a_partner(m, slot):
        p = zpos(slot)
        send(a_block(m, p), a_block(m, p), wp_s.at[m], wp_r.at[m, slot], partner, False)

    def a2_wait(m, r):
        for slot in slots_of(NZ, r):
            arrived(a_block(m, zpos(slot)), w_r2.at[m, slot, 0])

    def b1_send(m, r):
        ring_z(m, lambda p: w.at[m, p, y, 1], r, w_s1.at[m], lambda s: w_r1.at[m, s])

    def b1_wait(m, r):
        for slot in slots_of(NZ, r):
            arrived(w.at[m, zpos(slot), y, 1], w_r1.at[m, slot])

    def b2_send(m, slot, r):
        ring_y(m, zpos(slot), 1, r, w_s2.at[m], lambda s: w_r2.at[m, slot, s])

    def b_partner(m, slot, yslot):
        p = w.at[m, zpos(slot), ypos(yslot), 1]
        send(p, p, wp_s.at[m], wp_r.at[m, slot], partner, False)

    def b2_wait(m, slot, r):
        for yslot in slots_of(NY, r):
            arrived(w.at[m, zpos(slot), ypos(yslot), 1], w_r2.at[m, slot, yslot])
            b_partner(m, slot, yslot)

    RZ = NZ // 2
    RY = NY // 2

    def y_start():
        @core0
        def _():
            for m in range(3):
                a1_send(m, 1)

    def y_more(r):
        @core0
        def _():
            for m in range(3):
                a1_wait(m, r)
                if r < RY:
                    a1_send(m, r + 1)

    def z_start():
        @core0
        def _():
            for m in range(3):
                a2_send(m, 1)
            for m in range(3):
                a_partner(m, 0)

        @core1
        def _():
            for m in range(3):
                b1_send(m, 1)
            for m in range(3):
                b2_send(m, 0, 1)
                b_partner(m, 0, 0)

    def tick(r, ms=(0, 1, 2)):
        @core0
        def _():
            for m in ms:
                if r <= RZ:
                    a2_wait(m, r)
                    if r < RZ:
                        a2_send(m, r + 1)
                    for slot in slots_of(NZ, r):
                        a_partner(m, slot)

        @core1
        def _():
            for m in ms:
                if r <= RZ:
                    b1_wait(m, r)
                    if r < RZ:
                        b1_send(m, r + 1)
                    for slot in slots_of(NZ, r):
                        b2_send(m, slot, 1)
                        b_partner(m, slot, 0)
                for k in range(1, RY + 1):
                    if 0 <= r - k <= RZ:
                        for slot in slots_of(NZ, r - k):
                            b2_wait(m, slot, k)
                            if k < RY:
                                b2_send(m, slot, k + 1)

    y_start()

    lane = lax.broadcasted_iota(jnp.int32, (T, 256), 1)
    own0 = (lane < 64) | ((lane >= 128) & (lane < 160))
    own1 = ((lane >= 64) & (lane < 128)) | ((lane >= 160) & (lane < 192))
    own2 = ((lane >= 64) & (lane < 96)) | (lane >= 128)

    def spread(k):
        narrow = qall[k, :, 0:256]
        wide = qall[k, :, 128:384]
        zero = jnp.zeros_like(narrow)
        qx[0, k * T : (k + 1) * T, :] = jnp.where(own0, narrow, zero)
        qx[1, k * T : (k + 1) * T, :] = jnp.where(own1, narrow, zero)
        qx[2, k * T : (k + 1) * T, :] = jnp.where(own2, wide, zero)

    spread(0)
    mrow[...] = jnp.full_like(mrow, -1e30)
    lrow[...] = jnp.zeros_like(lrow)
    acc[...] = jnp.zeros_like(acc)
    for k in range(1, NY):
        arrived(qall.at[k], q_r.at[k])
        spread(k)

    QB = min(256, NY * T)
    head_rows = ((0, 64), (64, 128), (128, 256))

    def attend(first, count):
        nk = count * 2 * T
        k_narrow = kv[first : first + count, :, :, 0:256].reshape(nk, 256)
        k_wide = kv[first : first + count, :, :, 128:384].reshape(nk, 256)

        def values(h):
            lo, hi = ((384, 512), (384, 512), (512, 640))[h]
            r0, r1 = ((0, 64), (64, 128), (0, 128))[h]
            return jnp.concatenate(
                [kv[first + s, cc, r0:r1, lo:hi] for s in range(count) for cc in range(2)], axis=1
            )

        def block(b, carry):
            cols = pl.ds(pl.multiple_of(b * QB, QB), QB)
            for h in range(3):
                s = dot_nt(k_narrow if h < 2 else k_wide, qx[h, cols, :]) * (scales[h] * LOG2E)
                old = mrow[h : h + 1, cols]
                new = jnp.maximum(old, jnp.max(s, axis=0, keepdims=True))
                shrink = jnp.exp2(old - new)
                p = jnp.exp2(s - new)
                lrow[h : h + 1, cols] = lrow[h : h + 1, cols] * shrink + jnp.sum(p, axis=0, keepdims=True)
                mrow[h : h + 1, cols] = new
                r0, r1 = head_rows[h]
                acc[r0:r1, cols] = acc[r0:r1, cols] * shrink + dot(values(h), p.astype(BF16))
            return carry

        lax.fori_loop(0, NY * T // QB, block, 0)

    arrived(kv.at[0, 1 - c], kvp_r.at[0])
    attend(0, 1)
    y_more(1)
    if NX > 1:
        wo_wait(1)
        if 1 < NX // 2:
            wo_send(2)
    for r in range(1, RZ + 1):
        ring = slots_of(NZ, r)
        for slot in ring:
            arrived(kv.at[slot, c], kv_r.at[slot])
        if r < RZ:
            kv_send(r + 1)
        for slot in ring:
            kv_partner(slot)
        if r == max(RZ - 1, 1):
            for k in range(2, RY + 1):
                y_more(k)
            z_start()
        for slot in ring:
            arrived(kv.at[slot, 1 - c], kvp_r.at[slot])
        attend(ring[0], len(ring))

    for k in range(NY):
        cols = slice(k * T, (k + 1) * T)
        osend[k] = acc[:, cols].astype(BF16)
        ssend[k, 0:3] = mrow[0:3, cols]
        ssend[k, 3:6] = lrow[0:3, cols]
        ssend[k, 6:8] = jnp.zeros((2, T), F32)
    for k in range(1, NY):
        send(osend.at[k], orecv.at[NY - k], o_s.at[k], o_r.at[NY - k], dev(yy=y + k))
        send(ssend.at[k], srecv.at[NY - k], st_s.at[k], st_r.at[NY - k], dev(yy=y + k))
    for r in range(2, NX // 2 + 1):
        wo_wait(r)
        if r < NX // 2:
            wo_send(r + 1)
    for k in range(1, NY):
        arrived(orecv.at[k], o_r.at[k])
        arrived(srecv.at[k], st_r.at[k])
    ms = [ssend[0, 0:3]] + [srecv[k, 0:3] for k in range(1, NY)]
    ls = [ssend[0, 3:6]] + [srecv[k, 3:6] for k in range(1, NY)]
    top = functools.reduce(jnp.maximum, ms)
    ws = [jnp.exp2(m - top) for m in ms]
    total = sum(a * b for a, b in zip(ws, ls))
    outs = []
    for h in range(3):
        r0, r1 = head_rows[h]
        o = acc[r0:r1, 0:T] * ws[0][h : h + 1]
        for k in range(1, NY):
            o = o + orecv[k, r0:r1].astype(F32) * ws[k][h : h + 1]
        o = o / total[h : h + 1]
        outs.append(o * lax.rsqrt(jnp.mean(o * o, axis=0, keepdims=True) + EPS))
    heads = jnp.transpose(jnp.concatenate(outs, axis=0))
    mixed[x] = (heads * ogain_ref[...]).astype(BF16)
    for k in range(1, NX):
        send(mixed.at[x], mixed.at[x], mx_s.at[k], mx_r.at[NX - k], dev(xx=x + k))
    tick(1)
    for k in range(1, NX):
        p = (x + k) % NX
        arrived(mixed.at[p], mx_r.at[k])
        arrived(resid.at[p], re_r.at[k])
    for slot in range(1, NX):
        arrived(wo.at[(x + offset_of(NX, slot) + 2 * NX) % NX, 1 - c], wop_r.at[slot])
    mixed_all = jnp.concatenate([mixed[k] for k in range(NX)], axis=1)

    def project(n, squares):
        cols = pl.ds(pl.multiple_of(n * 256, 256), 256)
        s = dot(mixed_all, wo[:, :, :, cols].reshape(NX * 256, 256))
        s = (s + resid[:, :, cols].reshape(T, 256).astype(F32)).astype(BF16)
        mid[n] = s
        s = s.astype(F32)
        return squares + jnp.sum(s * s, axis=1, keepdims=True)

    squares = lax.fori_loop(0, D // 256, project, jnp.zeros((T, 1), F32))
    factor = lax.rsqrt(squares / D + EPS)

    def scale(n, carry):
        cols = pl.ds(pl.multiple_of(n * 256, 256), 256)
        normed[n] = (mid[n].astype(F32) * factor * mgain_ref[:, cols]).astype(BF16)
        return carry

    lax.fori_loop(0, D // 256, scale, 0)

    def from_partner(m, slot):
        arrived(w.at[m, zpos(slot), :, 1 - c], wp_r.at[m, slot])

    accg[...] = jnp.zeros_like(accg)
    accu[...] = jnp.zeros_like(accu)
    F = accg.shape[1]

    def widen(k):
        for slot in slots_of(NZ, k):
            from_partner(0, slot)
            from_partner(1, slot)
        ring = slots_of(NZ, k)

        def one(i, carry):
            step = 0 if k == 0 else (k if len(ring) == 1 else (2 * i - 1) * k)
            p = (z + step + 2 * NZ) % NZ
            n = normed[p]
            accg[...] += dot(n, w[0, p].reshape(256, F))
            accu[...] += dot(n, w[1, p].reshape(256, F))
            return carry

        lax.fori_loop(0, len(ring), one, 0)

    for r in range(2, RZ + RY + 1):
        tick(r)
        if r >= RY:
            widen(r - RY)
    for m in (2,):
        for slot in range(NZ):
            from_partner(m, slot)
    g = accg[...]
    hid[...] = (g / (1.0 + jnp.exp(-g)) * accu[...]).astype(BF16)
    GROUPS = rs_r.shape[0]
    per = NZ // GROUPS

    def narrow(n, carry):
        s = dot_nt(hid[...], w[2, n].reshape(256, F)).astype(BF16)
        part[n] = s.reshape(NX, R, 256)
        return carry

    for gr in range(GROUPS):
        lax.fori_loop(gr * per, (gr + 1) * per, narrow, 0)
        rows = pl.ds(gr * per, per)
        for k in range(1, NX):
            p = (x + k) % NX
            send(part.at[rows, p], rsum.at[NX - k, rows], rs_s.at[gr, k], rs_r.at[gr, NX - k], dev(xx=x + k))
    for gr in range(GROUPS):
        rows = pl.ds(gr * per, per)
        for k in range(1, NX):
            arrived(rsum.at[k, rows], rs_r.at[gr, k])
        for n in range(gr * per, (gr + 1) * per):
            s = part[n, x].astype(F32)
            for k in range(1, NX):
                s = s + rsum[k, n].astype(F32)
            s = s + mid[n, pl.ds(pl.multiple_of(x * R, R), R), :].astype(F32)
            out_ref[:, n * 256 : (n + 1) * 256] = s.astype(BF16)

    for d in pend:
        d.wait_send()

    @core0
    def _():
        for m in range(3):
            arrived(w.at[m, 0, pl.ds(0, NY - 1), 0], w_s1.at[m])
            arrived(w.at[m, pl.ds(0, NZ - 1), :, 0], w_s2.at[m])
            arrived(w.at[m, :, :, 0], wp_s.at[m])

    @core1
    def _():
        for m in range(3):
            arrived(w.at[m, pl.ds(0, NZ - 1), 0, 1], w_s1.at[m])
            arrived(w.at[m, :, pl.ds(0, NY - 1), 1], w_s2.at[m])
            arrived(w.at[m, :, :, 1], wp_s.at[m])


def on_device(
    NZ,
    NX,
    residual,
    query_content,
    query_rotary,
    key_latent,
    rotary_key,
    latent_gain,
    key_weight,
    value_weight,
    output_gain,
    output_weight,
    mixer_gain,
    gate_weight,
    up_weight,
    down_weight,
):
    T = key_latent.shape[0]
    R, D = residual.shape
    F = gate_weight.shape[1]
    positions = lax.axis_index("sp") * T + lax.iota(jnp.int32, T)
    lanes = jnp.arange(128) % ROT_DIM
    half = ROT_DIM // 2
    power = 2.0 * (lanes % half).astype(F32) / ROT_DIM
    inverse = 1.0 / jnp.power(ROPE_BASE, power)
    angles = positions.astype(F32)[:, None] * inverse[None, :]
    cos = jnp.cos(angles)
    sin = jnp.where(lanes[None, :] < half, -jnp.sin(angles), jnp.sin(angles))
    vm = pl.BlockSpec(memory_space=pltpu.VMEM)
    hbm = pl.BlockSpec(memory_space=pl.ANY)
    V = pltpu.VMEM
    S = pltpu.SemaphoreType.DMA
    scales = ((64 + ROT_DIM) ** -0.5,) * 2 + ((128 + ROT_DIM) ** -0.5,)
    return pl.pallas_call(
        functools.partial(kernel, NZ, NX, scales),
        out_shape=jax.ShapeDtypeStruct((R, D), BF16),
        in_specs=[vm] * 11 + [hbm] * 5,
        out_specs=vm,
        scratch_shapes=[
            V((3, NZ, NY, 2, R, F), BF16),
            V((NZ, 2, T, 640), BF16),
            V((NY, T, 384), BF16),
            V((3, NY * T, 256), BF16),
            V((256, NY * T), F32),
            V((8, NY * T), F32),
            V((8, NY * T), F32),
            V((NY, 256, T), BF16),
            V((NY, 256, T), BF16),
            V((NY, 8, T), F32),
            V((NY, 8, T), F32),
            V((NX, T, 256), BF16),
            V((NX, 2, 128, D), BF16),
            V((NX, R, D), BF16),
            V((NZ, T, 256), BF16),
            V((NZ, T, 256), BF16),
            V((T, F), F32),
            V((T, F), F32),
            V((T, F), BF16),
            V((NZ, NX, R, 256), BF16),
            V((NX, NZ, R, 256), BF16),
            S((5,)),
            S((NZ,)),
            S((NZ,)),
            S((NZ,)),
            S((NZ,)),
            S((NY,)),
            S((NY,)),
            S((NY,)),
            S((NY,)),
            S((NY,)),
            S((NY,)),
            S((NX,)),
            S((NX,)),
            S((NX,)),
            S((NX,)),
            S((NX,)),
            S((NX,)),
            S((NX,)),
            S((NX,)),
            S((NZ // 2, NX)),
            S((NZ // 2, NX)),
            S((3,)),
            S((3,)),
            S((3,)),
            S((3, NZ)),
            S((3, NZ, NY)),
            S((3, NZ)),
        ],
        compiler_params=pltpu.CompilerParams(
            collective_id=0, has_side_effects=True, vmem_limit_bytes=60 * 1024 * 1024
        ),
    )(
        cos,
        sin,
        query_content,
        query_rotary,
        key_latent,
        rotary_key,
        latent_gain[None, :],
        key_weight,
        value_weight,
        output_gain[None, :],
        mixer_gain[None, :],
        residual,
        output_weight.reshape(2, 128, D),
        gate_weight,
        up_weight,
        down_weight.T,
    )


def solution(mesh):
    placed = (
        P(("sp", "tp"), None),
        P("sp", "tp"),
        P("sp", "tp"),
        P("sp", None),
        P("sp", None),
        P(),
        P(None, "tp"),
        P(None, "tp"),
        P("tp"),
        P("tp", None),
        P(),
        P("sp", "tp"),
        P("sp", "tp"),
        P("tp", "sp"),
    )
    NZ = mesh.shape["sp"] // (2 * NY)
    NX = mesh.shape["tp"]
    return jax.shard_map(
        functools.partial(on_device, NZ, NX),
        mesh=mesh,
        in_specs=placed,
        out_specs=P(("sp", "tp"), None),
        check_vma=False,
    )
```

time: 235 us -> 115 us (0.49)
  waiting for transfers between devices: 131 us -> 0 us
  Pallas kernels: 0 us -> 110 us
  blocking collectives: 36.7 us -> 0 us
  matrix products: 29.5 us -> 0 us
  between operations: 13.6 us -> 0.03 us
  local copies, waits for them, and re-layouts: 14.3 us -> 3.71 us
  other arithmetic: 8.62 us -> 0.99 us
    all_gather x2 -> x0, waiting for transfers between devices: 131 us -> none  [the longest x1 86.9 us: side_by_side(): filled = lax.all_gather(both, axis, axis=dim, tiled=True)]
    pallas_call x0 -> x1, Pallas kernels: none -> 110 us  [on_device(): pl.pallas_call(functools.partial(kernel, NZ, NX, scales), out_shape=jax.S...]
    dot_general x11 -> x0, matrix products: 29.5 us -> none  [the longest x1 7.23 us: on_device(): jnp.dot(hidden, down_whole, preferred_element_type=jnp.float32)]
    all_to_all x2 -> x0, blocking collectives: 25.7 us -> none  [summed_on_arrival(): lax.all_to_all(pieces, axis, split_axis=0, concat_axis=0, tiled=True)]
    slice x5 -> x0, local copies, waits for them, and re-layouts: 13.5 us -> none  [the longest x2 8.56 us: on_device(): piece_keys[:, :narrow_cols].reshape(length, narrow_dev, NARROW_DIM)]
    all_gather x1 -> x0, blocking collectives: 11 us -> none  [on_device(): block_normed = lax.all_gather(normed, 'tp', axis=0, tiled=True)]
    reduce_sum x6 -> x0, other arithmetic: 3.55 us -> none  [the longest x2 2.22 us: group_update(): totals = totals * shrink + jnp.sum(powers, axis=-1)]
    unnamed x12 -> x7, local copies, waits for them, and re-layouts: 0.49 us -> 3.71 us
  transfers between devices with their start and end apart: 2 -> 0, of which waited for: 2 -> 0; matrix products, arithmetic and copies ran while one was open for 15% -> 0% of each run, Pallas kernels for 0% -> 0%
where the time goes in v1:
time: 115 us
  Pallas kernels  110 us (96%)
  local copies, waits for them, and re-layouts  3.71 us (3%)
    pallas_call x1, Pallas kernels, on_device(): pl.pallas_call(functools.partial(kernel, NZ, NX, scales), out_shape=jax.S...  110 us
    unnamed x7, local copies, waits for them, and re-layouts  3.71 us

profile of v1, /device:TPU:1, one launch (start us, length us, event | category | flops | bytes accessed | tf_op | source)
XLA Modules:
  0.0 114.8 jit_solution(1652135748110297603)
XLA Ops:
  0.0 0.0 copy-start
  0.0 0.7 copy-done
  0.7 0.0 copy-start.1
  0.7 0.7 copy.15.qr_ref
  1.5 0.0 copy-done.1
  1.5 0.7 copy.16.rk_ref
  2.2 1.0 negate_select_fusion
  3.1 110.1 %shard_map.136 = bf16[32,2048]{1,0:T(8,128)(2,1)} custom-call(f32[128,128]{1,0:T(8,128)} %get-tuple-element.6.cos_ref, f32[128,128]{1,0:T(8,128)} %get-tuple-element.5.sin_ref, bf16[128,256]{1,0:T(8,128)(2,1)} %qc_ref.1, bf16[128,96]{1,0:T(8,128)(2,1)} %copy.15.qr_ref, bf16[128,512]{1,0:T(8,128)(2,1)} %lat_ref.1, bf16[128,32]{1,0:T(8,128)(2,1)} %copy.16.rk_ref, ...), custom_call_target="tpu_custom_call" | custom-call | tf_op jit(solution)/shard_map/pallas_call | solution.py:621
  113.2 1.6 %copy.18 = bf16[32,2048]{1,0:T(8,128)(2,1)} copy(bf16[32,2048]{1,0:T(8,128)(2,1)} %shard_map.136) | data formatting | bytes 262144
  (3 shorter events, 0.0 us)
Async XLA Ops:
  0.0 0.7 copy-start
  0.7 0.7 copy-start.1

commit v2 on v1

--- a/solution.py
+++ b/solution.py
@@ -1,3 +1,4 @@
+import contextlib
 import functools
 
 import jax
@@ -36,21 +37,27 @@
     scales,
     cos_ref,
     sin_ref,
-    qc_ref,
-    qr_ref,
-    lat_ref,
-    rk_ref,
-    lgain_ref,
-    kw_ref,
-    vw_ref,
     ogain_ref,
     mgain_ref,
+    lgain_ref,
+    lat_hbm,
+    kw_hbm,
+    vw_hbm,
+    qc_hbm,
+    qr_hbm,
+    rk_hbm,
     resid_hbm,
     ow_hbm,
     gate_hbm,
     up_hbm,
     down_hbm,
     out_ref,
+    lat_ref,
+    kw_ref,
+    vw_ref,
+    qc_ref,
+    qr_ref,
+    rk_ref,
     w,
     kv,
     qall,
@@ -108,6 +115,12 @@
     T = qc_ref.shape[0]
     R = resid.shape[1]
     D = resid.shape[2]
+    phases = contextlib.ExitStack()
+
+    def phase(name):
+        phases.close()
+        phases.enter_context(jax.named_scope(name))
+
     pend = []
 
     def dev(zz=None, yy=None, cc=None, xx=None):
@@ -140,16 +153,6 @@
     yboth, ylast = hops(NY)
     xboth, xlast = hops(NX)
 
-    loc = [
-        pltpu.make_async_copy(resid_hbm, resid.at[x], loc_sem.at[0]),
-        pltpu.make_async_copy(ow_hbm, wo.at[x], loc_sem.at[1]),
-        pltpu.make_async_copy(gate_hbm, w.at[0, z, y, c], loc_sem.at[2]),
-        pltpu.make_async_copy(up_hbm, w.at[1, z, y, c], loc_sem.at[3]),
-        pltpu.make_async_copy(down_hbm, w.at[2, z, y, c], loc_sem.at[4]),
-    ]
-    for d in loc:
-        d.start()
-
     barrier = pltpu.get_barrier_semaphore()
     peers = [partner]
     peers += [dev(zz=z + 1)] + ([dev(zz=z - 1)] if NZ > 2 else [])
@@ -158,37 +161,61 @@
     for p in peers:
         pl.semaphore_signal(barrier, inc=1, device_id=p, device_id_type=MESH)
 
-    lane_q = lax.broadcasted_iota(jnp.int32, (qr_ref.shape[1], 128), 1)
-    row_q = lax.broadcasted_iota(jnp.int32, (qr_ref.shape[1], 128), 0)
+    def local(pairs, first):
+        copies = [
+            pltpu.make_async_copy(a, b, loc_sem.at[first + k]) for k, (a, b) in enumerate(pairs)
+        ]
+        for d in copies:
+            d.start()
+        return copies
+
+    small = local(
+        [(lat_hbm, lat_ref), (kw_hbm, kw_ref), (vw_hbm, vw_ref), (qc_hbm, qc_ref), (qr_hbm, qr_ref), (rk_hbm, rk_ref)],
+        0,
+    )
+    loc = local(
+        [
+            (gate_hbm, w.at[0, z, y, c]),
+            (up_hbm, w.at[1, z, y, c]),
+            (down_hbm, w.at[2, z, y, c]),
+            (ow_hbm, wo.at[x]),
+            (resid_hbm, resid.at[x]),
+        ],
+        6,
+    )
+
+    phase("qkv")
+    for d in small:
+        d.wait()
     half = ROT_DIM // 2
-    swapped_q = jnp.where(lane_q % ROT_DIM < half, lane_q + half, lane_q - half)
-    qr = qr_ref[...]
-    q_same = dot(qr, (row_q == lane_q).astype(BF16))
-    q_swap = dot(qr, (row_q == swapped_q).astype(BF16))
     cos = cos_ref[...]
     sin = sin_ref[...]
-    qall[0, :, 0:128] = qc_ref[:, 0:128]
-    qall[0, :, 128:256] = (q_same * cos + q_swap * sin).astype(BF16)
-    qall[0, :, 256:384] = qc_ref[:, 128:256]
-
-    lane_k = lax.broadcasted_iota(jnp.int32, (ROT_DIM, 128), 1)
-    row_k = lax.broadcasted_iota(jnp.int32, (ROT_DIM, 128), 0)
-    lane_in = lane_k % ROT_DIM
-    swapped_k = jnp.where(lane_in < half, lane_in + half, lane_in - half)
-    rk = rk_ref[...]
-    k_same = dot(rk, (row_k == lane_in).astype(BF16))
-    k_swap = dot(rk, (row_k == swapped_k).astype(BF16))
+
+    def turned(ref, count):
+        rows = []
+        for h in range(count):
+            a = ref[h * ROT_DIM : h * ROT_DIM + half, :].astype(F32)
+            b = ref[h * ROT_DIM + half : (h + 1) * ROT_DIM, :].astype(F32)
+            rows += [a * cos - b * sin, b * cos + a * sin]
+        return rows
+
     lat = lat_ref[...].astype(F32)
     lat = lat * lax.rsqrt(jnp.mean(lat * lat, axis=-1, keepdims=True) + EPS)
     lat = (lat * lgain_ref[...]).astype(BF16)
     keys = dot(lat, kw_ref[...]).astype(BF16)
     vals = jnp.transpose(dot(lat, vw_ref[...])).astype(BF16)
     kv[0, c, :, 0:128] = keys[:, 0:128]
-    kv[0, c, :, 128:256] = (k_same * cos + k_swap * sin).astype(BF16)
+    kv[0, c, :, 128:256] = jnp.transpose(jnp.concatenate(turned(rk_ref, 1) * 4, axis=0)).astype(BF16)
     kv[0, c, :, 256:384] = keys[:, 128:256]
     kv[0, c, :, 384:512] = vals[0:128, :]
     kv[0, c, :, 512:640] = vals[128:256, :]
 
+    turned_q = turned(qr_ref, 3) + [jnp.zeros((ROT_DIM, T), F32)]
+    qall[0, :, 0:128] = qc_ref[:, 0:128]
+    qall[0, :, 128:256] = jnp.transpose(jnp.concatenate(turned_q, axis=0)).astype(BF16)
+    qall[0, :, 256:384] = qc_ref[:, 128:256]
+
+    phase("barrier")
     pl.semaphore_wait(barrier, len(peers))
 
     def kv_copy(src_slot, dst_slot, device):
@@ -222,14 +249,6 @@
 
     def ypos(slot):
         return (y + offset_of(NY, slot) + 2 * NY) % NY
-
-    kv_send(1)
-    kv_partner(0)
-    for k in range(1, NY):
-        send(qall.at[0], qall.at[NY - k], q_s.at[k], q_r.at[NY - k], dev(yy=y + k))
-
-    for d in loc:
-        d.wait()
 
     def wo_send(r):
         if r in xboth:
@@ -244,11 +263,6 @@
             p = (x + offset_of(NX, slot) + 2 * NX) % NX
             arrived(wo.at[p, c], wo_r.at[slot])
             send(wo.at[p, c], wo.at[p, c], wop_s.at[slot], wop_r.at[slot], partner)
-
-    for k in range(1, NX):
-        send(resid.at[x], resid.at[x], re_s.at[k], re_r.at[NX - k], dev(xx=x + k))
-    if NX > 1:
-        wo_send(1)
 
     def zdir(m):
         return dirc * (1 - 2 * (m % 2))
@@ -293,86 +307,81 @@
             arrived(a_block(m, zpos(slot)), w_r2.at[m, slot, 0])
 
     def b1_send(m, r):
-        ring_z(m, lambda p: w.at[m, p, y, 1], r, w_s1.at[m], lambda s: w_r1.at[m, s])
+        ring_z(m, lambda p: w.at[m, p, y, c], r, w_s1.at[m], lambda s: w_r1.at[m, s])
 
     def b1_wait(m, r):
         for slot in slots_of(NZ, r):
-            arrived(w.at[m, zpos(slot), y, 1], w_r1.at[m, slot])
+            arrived(w.at[m, zpos(slot), y, c], w_r1.at[m, slot])
 
     def b2_send(m, slot, r):
-        ring_y(m, zpos(slot), 1, r, w_s2.at[m], lambda s: w_r2.at[m, slot, s])
+        ring_y(m, zpos(slot), c, r, w_s2.at[m], lambda s: w_r2.at[m, slot, s])
 
     def b_partner(m, slot, yslot):
-        p = w.at[m, zpos(slot), ypos(yslot), 1]
+        p = w.at[m, zpos(slot), ypos(yslot), c]
         send(p, p, wp_s.at[m], wp_r.at[m, slot], partner, False)
-
-    def b2_wait(m, slot, r):
-        for yslot in slots_of(NY, r):
-            arrived(w.at[m, zpos(slot), ypos(yslot), 1], w_r2.at[m, slot, yslot])
-            b_partner(m, slot, yslot)
 
     RZ = NZ // 2
     RY = NY // 2
 
-    def y_start():
-        @core0
-        def _():
-            for m in range(3):
-                a1_send(m, 1)
-
-    def y_more(r):
-        @core0
-        def _():
-            for m in range(3):
-                a1_wait(m, r)
-                if r < RY:
-                    a1_send(m, r + 1)
-
-    def z_start():
-        @core0
-        def _():
-            for m in range(3):
-                a2_send(m, 1)
-            for m in range(3):
-                a_partner(m, 0)
-
-        @core1
-        def _():
-            for m in range(3):
-                b1_send(m, 1)
-            for m in range(3):
-                b2_send(m, 0, 1)
-                b_partner(m, 0, 0)
-
-    def tick(r, ms=(0, 1, 2)):
-        @core0
-        def _():
-            for m in ms:
-                if r <= RZ:
-                    a2_wait(m, r)
-                    if r < RZ:
-                        a2_send(m, r + 1)
-                    for slot in slots_of(NZ, r):
-                        a_partner(m, slot)
-
-        @core1
-        def _():
-            for m in ms:
-                if r <= RZ:
-                    b1_wait(m, r)
-                    if r < RZ:
-                        b1_send(m, r + 1)
-                    for slot in slots_of(NZ, r):
-                        b2_send(m, slot, 1)
-                        b_partner(m, slot, 0)
-                for k in range(1, RY + 1):
-                    if 0 <= r - k <= RZ:
-                        for slot in slots_of(NZ, r - k):
-                            b2_wait(m, slot, k)
-                            if k < RY:
-                                b2_send(m, slot, k + 1)
-
-    y_start()
+    def b_start(m):
+        b1_send(m, 1)
+        b2_send(m, 0, 1)
+        b_partner(m, 0, 0)
+
+    def b_z(m, r):
+        b1_wait(m, r)
+        if r < RZ:
+            b1_send(m, r + 1)
+        for slot in slots_of(NZ, r):
+            b2_send(m, slot, 1)
+            b_partner(m, slot, 0)
+
+    def b_y(m, r, k):
+        for slot in slots_of(NZ, r):
+            for yslot in slots_of(NY, k):
+                arrived(w.at[m, zpos(slot), ypos(yslot), c], w_r2.at[m, slot, yslot])
+            if k < RY:
+                b2_send(m, slot, k + 1)
+            for yslot in slots_of(NY, k):
+                b_partner(m, slot, yslot)
+
+    def a_y(m, k):
+        a1_wait(m, k)
+        if k < RY:
+            a1_send(m, k + 1)
+
+    def a_z(m, r):
+        a2_wait(m, r)
+        if r < RZ:
+            a2_send(m, r + 1)
+        for slot in slots_of(NZ, r):
+            a_partner(m, slot)
+
+    def on(core, *steps):
+        def run():
+            for f, *a in steps:
+                f(*a)
+
+        if core is None:
+            run()
+        else:
+            pl.when(c == core)(run)
+
+    def both01(f, *a):
+        return [(f, 0, *a), (f, 1, *a)]
+
+    phase("send0")
+    kv_send(1)
+    kv_partner(0)
+    for k in range(1, NY):
+        send(qall.at[0], qall.at[NY - k], q_s.at[k], q_r.at[NY - k], dev(yy=y + k))
+    for d in loc:
+        d.wait()
+    on(0, *both01(a1_send, 1))
+    on(1, *both01(b_start))
+    wo_send(1)
+    for k in range(1, NX):
+        send(resid.at[x], resid.at[x], re_s.at[k], re_r.at[NX - k], dev(xx=x + k))
 
     lane = lax.broadcasted_iota(jnp.int32, (T, 256), 1)
     own0 = (lane < 64) | ((lane >= 128) & (lane < 160))
@@ -387,10 +396,25 @@
         qx[1, k * T : (k + 1) * T, :] = jnp.where(own1, narrow, zero)
         qx[2, k * T : (k + 1) * T, :] = jnp.where(own2, wide, zero)
 
+    def kv_wait(r):
+        phase(f"kvw#r={r}")
+        for slot in slots_of(NZ, r):
+            arrived(kv.at[slot, c], kv_r.at[slot])
+        if r < RZ:
+            kv_send(r + 1)
+        for slot in slots_of(NZ, r):
+            kv_partner(slot)
+
+    phase("spread0")
     spread(0)
     mrow[...] = jnp.full_like(mrow, -1e30)
     lrow[...] = jnp.zeros_like(lrow)
     acc[...] = jnp.zeros_like(acc)
+    kv_wait(1)
+    phase("g1")
+    on(1, *both01(b_z, 1))
+    on(0, *both01(a_y, 1))
+    phase("qwait")
     for k in range(1, NY):
         arrived(qall.at[k], q_r.at[k])
         spread(k)
@@ -426,29 +450,39 @@
 
         lax.fori_loop(0, NY * T // QB, block, 0)
 
-    arrived(kv.at[0, 1 - c], kvp_r.at[0])
-    attend(0, 1)
-    y_more(1)
-    if NX > 1:
-        wo_wait(1)
-        if 1 < NX // 2:
-            wo_send(2)
-    for r in range(1, RZ + 1):
+    def att(r):
+        phase(f"attw#r={r}")
         ring = slots_of(NZ, r)
         for slot in ring:
-            arrived(kv.at[slot, c], kv_r.at[slot])
-        if r < RZ:
-            kv_send(r + 1)
-        for slot in ring:
-            kv_partner(slot)
-        if r == max(RZ - 1, 1):
-            for k in range(2, RY + 1):
-                y_more(k)
-            z_start()
-        for slot in ring:
             arrived(kv.at[slot, 1 - c], kvp_r.at[slot])
+        phase(f"att#r={r}")
         attend(ring[0], len(ring))
 
+    att(0)
+    kv_wait(2)
+    phase("g2")
+    on(0, *both01(a_y, 2), (a2_send, 0, 1), (a_partner, 0, 0), (a_partner, 1, 0))
+    on(1, *both01(b_y, 0, 1))
+    on(None, (b_start, 2))
+    att(1)
+    kv_wait(3)
+    phase("g3")
+    on(0, (a2_send, 1, 1))
+    on(1, *both01(b_z, 2), *both01(b_y, 0, 2), *both01(b_y, 1, 1))
+    on(None, (b_z, 2, 1))
+    att(2)
+    kv_wait(4)
+    phase("g4")
+    on(0, *both01(a_z, 1))
+    on(1, *both01(b_y, 1, 2), *both01(b_y, 2, 1))
+    on(None, (b_y, 2, 0, 1))
+    att(3)
+    phase("g5")
+    on(1, *both01(b_z, 3))
+    on(None, (b_z, 2, 2), (b_y, 2, 0, 2), (b_y, 2, 1, 1))
+    att(4)
+
+    phase("osend")
     for k in range(NY):
         cols = slice(k * T, (k + 1) * T)
         osend[k] = acc[:, cols].astype(BF16)
@@ -458,13 +492,15 @@
     for k in range(1, NY):
         send(osend.at[k], orecv.at[NY - k], o_s.at[k], o_r.at[NY - k], dev(yy=y + k))
         send(ssend.at[k], srecv.at[NY - k], st_s.at[k], st_r.at[NY - k], dev(yy=y + k))
-    for r in range(2, NX // 2 + 1):
-        wo_wait(r)
-        if r < NX // 2:
-            wo_send(r + 1)
+    phase("g6")
+    on(1, *both01(b_y, 2, 2), *both01(b_y, 3, 1))
+    wo_wait(1)
+    wo_send(2)
+    phase("owait")
     for k in range(1, NY):
         arrived(orecv.at[k], o_r.at[k])
         arrived(srecv.at[k], st_r.at[k])
+    phase("merge")
     ms = [ssend[0, 0:3]] + [srecv[k, 0:3] for k in range(1, NY)]
     ls = [ssend[0, 3:6]] + [srecv[k, 3:6] for k in range(1, NY)]
     top = functools.reduce(jnp.maximum, ms)
@@ -482,13 +518,19 @@
     mixed[x] = (heads * ogain_ref[...]).astype(BF16)
     for k in range(1, NX):
         send(mixed.at[x], mixed.at[x], mx_s.at[k], mx_r.at[NX - k], dev(xx=x + k))
-    tick(1)
+    phase("g7")
+    on(0, *both01(a_z, 2))
+    on(1, *both01(b_z, 4), *both01(b_y, 3, 2))
+    on(None, (b_z, 2, 3), (b_y, 2, 1, 2), (b_y, 2, 2, 1))
+    wo_wait(2)
+    phase("mixw")
     for k in range(1, NX):
         p = (x + k) % NX
         arrived(mixed.at[p], mx_r.at[k])
         arrived(resid.at[p], re_r.at[k])
     for slot in range(1, NX):
         arrived(wo.at[(x + offset_of(NX, slot) + 2 * NX) % NX, 1 - c], wop_r.at[slot])
+    phase("proj")
     mixed_all = jnp.concatenate([mixed[k] for k in range(NX)], axis=1)
 
     def project(n, squares):
@@ -509,6 +551,7 @@
 
     lax.fori_loop(0, D // 256, scale, 0)
 
+    phase("mlp0")
     def from_partner(m, slot):
         arrived(w.at[m, zpos(slot), :, 1 - c], wp_r.at[m, slot])
 
@@ -532,56 +575,88 @@
 
         lax.fori_loop(0, len(ring), one, 0)
 
-    for r in range(2, RZ + RY + 1):
-        tick(r)
-        if r >= RY:
-            widen(r - RY)
-    for m in (2,):
-        for slot in range(NZ):
-            from_partner(m, slot)
+    phase("widen01")
+    widen(0)
+    widen(1)
+    phase("g8")
+    on(0, *both01(a_z, 3))
+    on(1, *both01(b_y, 4, 1))
+    on(None, (b_z, 2, 4), (b_y, 2, 2, 2), (b_y, 2, 3, 1))
+    phase("widen2")
+    widen(2)
+    phase("g9")
+    on(0, *both01(a_z, 4))
+    on(1, *both01(b_y, 4, 2))
+    phase("widen34")
+    widen(3)
+    widen(4)
+    phase("silu")
     g = accg[...]
     hid[...] = (g / (1.0 + jnp.exp(-g)) * accu[...]).astype(BF16)
-    GROUPS = rs_r.shape[0]
-    per = NZ // GROUPS
-
-    def narrow(n, carry):
-        s = dot_nt(hid[...], w[2, n].reshape(256, F)).astype(BF16)
-        part[n] = s.reshape(NX, R, 256)
+
+    def narrow(slot, carry):
+        p = (z + ((slot + 1) // 2) * (1 - 2 * (slot % 2)) + 2 * NZ) % NZ
+        s = dot_nt(hid[...], w[2, p].reshape(256, F)).astype(BF16)
+        part[slot] = s.reshape(NX, R, 256)
         return carry
 
-    for gr in range(GROUPS):
-        lax.fori_loop(gr * per, (gr + 1) * per, narrow, 0)
-        rows = pl.ds(gr * per, per)
+    def down(first, count):
+        for slot in range(first, first + count):
+            from_partner(2, slot)
+        lax.fori_loop(first, first + count, narrow, 0)
+
+    def sums_send(gr):
+        rows = pl.ds(2 * gr, 2)
         for k in range(1, NX):
             p = (x + k) % NX
             send(part.at[rows, p], rsum.at[NX - k, rows], rs_s.at[gr, k], rs_r.at[gr, NX - k], dev(xx=x + k))
-    for gr in range(GROUPS):
-        rows = pl.ds(gr * per, per)
+
+    phase("down0")
+    down(0, 4)
+    sums_send(0)
+    sums_send(1)
+    phase("g10")
+    on(None, (b_y, 2, 3, 2), (b_y, 2, 4, 1))
+    phase("down4")
+    down(4, 2)
+    sums_send(2)
+    phase("g11")
+    on(None, (b_y, 2, 4, 2))
+    phase("down6")
+    down(6, 2)
+    sums_send(3)
+    phase("final")
+    for gr in range(NZ // 2):
+        rows = pl.ds(2 * gr, 2)
         for k in range(1, NX):
             arrived(rsum.at[k, rows], rs_r.at[gr, k])
-        for n in range(gr * per, (gr + 1) * per):
-            s = part[n, x].astype(F32)
+        for slot in (2 * gr, 2 * gr + 1):
+            p = zpos(slot)
+            s = part[slot, x].astype(F32)
             for k in range(1, NX):
-                s = s + rsum[k, n].astype(F32)
-            s = s + mid[n, pl.ds(pl.multiple_of(x * R, R), R), :].astype(F32)
-            out_ref[:, n * 256 : (n + 1) * 256] = s.astype(BF16)
-
+                s = s + rsum[k, slot].astype(F32)
+            s = s + mid[p, pl.ds(pl.multiple_of(x * R, R), R), :].astype(F32)
+            out_ref[:, pl.ds(pl.multiple_of(p * 256, 256), 256)] = s.astype(BF16)
+
+    phase("sendw")
     for d in pend:
         d.wait_send()
 
-    @core0
-    def _():
-        for m in range(3):
-            arrived(w.at[m, 0, pl.ds(0, NY - 1), 0], w_s1.at[m])
-            arrived(w.at[m, pl.ds(0, NZ - 1), :, 0], w_s2.at[m])
-            arrived(w.at[m, :, :, 0], wp_s.at[m])
-
-    @core1
-    def _():
-        for m in range(3):
-            arrived(w.at[m, pl.ds(0, NZ - 1), 0, 1], w_s1.at[m])
-            arrived(w.at[m, :, pl.ds(0, NY - 1), 1], w_s2.at[m])
-            arrived(w.at[m, :, :, 1], wp_s.at[m])
+    def sent_a(m):
+        arrived(w.at[m, 0, pl.ds(0, NY - 1), 0], w_s1.at[m])
+        arrived(w.at[m, pl.ds(0, NZ - 1), :, 0], w_s2.at[m])
+        arrived(w.at[m, :, :, 0], wp_s.at[m])
+
+    def sent_b(m):
+        arrived(w.at[m, pl.ds(0, NZ - 1), 0, 1], w_s1.at[m])
+        arrived(w.at[m, :, pl.ds(0, NY - 1), 1], w_s2.at[m])
+        arrived(w.at[m, :, :, 1], wp_s.at[m])
+
+    on(0, (sent_a, 0), (sent_a, 1))
+    on(1, (sent_b, 0), (sent_b, 1))
+    on(None, (sent_b, 2))
+
+    phases.close()
 
 
 def on_device(
@@ -606,13 +681,11 @@
     R, D = residual.shape
     F = gate_weight.shape[1]
     positions = lax.axis_index("sp") * T + lax.iota(jnp.int32, T)
-    lanes = jnp.arange(128) % ROT_DIM
-    half = ROT_DIM // 2
-    power = 2.0 * (lanes % half).astype(F32) / ROT_DIM
+    power = jnp.arange(0, ROT_DIM, 2, dtype=F32) / ROT_DIM
     inverse = 1.0 / jnp.power(ROPE_BASE, power)
-    angles = positions.astype(F32)[:, None] * inverse[None, :]
+    angles = positions.astype(F32)[None, :] * inverse[:, None]
     cos = jnp.cos(angles)
-    sin = jnp.where(lanes[None, :] < half, -jnp.sin(angles), jnp.sin(angles))
+    sin = jnp.sin(angles)
     vm = pl.BlockSpec(memory_space=pltpu.VMEM)
     hbm = pl.BlockSpec(memory_space=pl.ANY)
     V = pltpu.VMEM
@@ -621,9 +694,15 @@
     return pl.pallas_call(
         functools.partial(kernel, NZ, NX, scales),
         out_shape=jax.ShapeDtypeStruct((R, D), BF16),
-        in_specs=[vm] * 11 + [hbm] * 5,
+        in_specs=[vm] * 5 + [hbm] * 11,
         out_specs=vm,
         scratch_shapes=[
+            V((T, key_latent.shape[1]), BF16),
+            V(key_weight.shape, BF16),
+            V(value_weight.shape, BF16),
+            V((T, 256), BF16),
+            V((query_rotary.shape[1], T), BF16),
+            V((ROT_DIM, T), BF16),
             V((3, NZ, NY, 2, R, F), BF16),
             V((NZ, 2, T, 640), BF16),
             V((NY, T, 384), BF16),
@@ -645,7 +724,7 @@
             V((T, F), BF16),
             V((NZ, NX, R, 256), BF16),
             V((NX, NZ, R, 256), BF16),
-            S((5,)),
+            S((11,)),
             S((NZ,)),
             S((NZ,)),
             S((NZ,)),
@@ -679,15 +758,15 @@
     )(
         cos,
         sin,
-        query_content,
-        query_rotary,
+        output_gain[None, :],
+        mixer_gain[None, :],
+        latent_gain[None, :],
         key_latent,
-        rotary_key,
-        latent_gain[None, :],
         key_weight,
         value_weight,
-        output_gain[None, :],
-        mixer_gain[None, :],
+        query_content,
+        query_rotary.T,
+        rotary_key.T,
         residual,
         output_weight.reshape(2, 128, D),
         gate_weight,

time: 115 us -> 93.2 us (0.81)
  Pallas kernels: 110 us -> 90.4 us
  local copies, waits for them, and re-layouts: 3.71 us -> 1.57 us
    pallas_call x1, Pallas kernels: 110 us -> 90.4 us  [on_device(): pl.pallas_call(functools.partial(kernel, NZ, NX, scales), out_shape=jax.S...]
    unnamed x7 -> x1, local copies, waits for them, and re-layouts: 3.71 us -> 1.57 us
where the time goes in v2:
time: 93.2 us; the launch traced here: 92.7 us
  Pallas kernels  90.4 us (97%)
  local copies, waits for them, and re-layouts  1.57 us (2%)
    pallas_call x1, Pallas kernels, on_device(): pl.pallas_call(functools.partial(kernel, NZ, NX, scales), out_shape=jax.S...  90.4 us

profile of v2, /device:TPU:1, one launch (start us, length us, event | category | flops | bytes accessed | tf_op | source)
XLA Modules:
  0.0 92.7 jit_solution(13717836326393372829)
XLA Ops:
  0.0 0.7 multiply_sine_fusion
  0.7 90.4 %shard_map.136 = bf16[32,2048]{1,0:T(8,128)(2,1)} custom-call(f32[16,128]{1,0:T(8,128)} %get-tuple-element.6.cos_ref, f32[16,128]{1,0:T(8,128)} %get-tuple-element.5.sin_ref, f32[1,256]{1,0:T(1,128)} %bitcast.13, f32[1,2048]{1,0:T(1,128)} %bitcast.10, f32[1,512]{1,0:T(1,128)} %bitcast.12, bf16[128,512]{1,0:T(8,128)(2,1)} %lat_hbm.1, ...), custom_call_target="tpu_custom_call" | custom-call | tf_op jit(solution)/shard_map/pallas_call | solution.py:694
  91.2 1.6 %copy.16 = bf16[32,2048]{1,0:T(8,128)(2,1)} copy(bf16[32,2048]{1,0:T(8,128)(2,1)} %shard_map.136) | data formatting | bytes 262144
  (2 shorter events, 0.0 us)

commit v3 on v2

--- a/solution.py
+++ b/solution.py
@@ -16,6 +16,90 @@
 MESH = pl.DeviceIdType.MESH
 F32 = jnp.float32
 BF16 = jnp.bfloat16
+
+PARTS = (
+    "kvw1",
+    "q1",
+    "q2",
+    "att0",
+    "kvw2",
+    "att1",
+    "kvw3",
+    "att2",
+    "kvw4",
+    "att3",
+    "att4",
+    "owait",
+    "mixw",
+    "widen0",
+    "widen1",
+    "widen2",
+    "widen3",
+    "widen4",
+    "hid",
+    "down0",
+    "down1",
+    "down2",
+    "down3",
+    "down4",
+    "final",
+)
+PLAN = (
+    (
+        (("ast", 0), ("by0", 2), ("ast", 1), ("bz0", 2),),
+        (),
+        (("zz", 2, 1), ("zy", 2, 1),),
+        (("ay", 1, 1),),
+        (("wo0",),),
+        (("y", 2, 1, 1), ("ay", 1, 2),),
+        (),
+        (("y", 2, 0, 1), ("re",), ("az0", 1),),
+        (("ay", 0, 1), ("zz", 2, 2), ("zy", 2, 2),),
+        (("ay", 0, 2), ("az0", 0),),
+        (("wo1",), ("az", 1, 1),),
+        (("az", 0, 1), ("az", 1, 2), ("wo2",),),
+        (("az", 0, 2), ("y", 2, 2, 1),),
+        (),
+        (("y", 2, 0, 2), ("zz", 2, 3), ("zy", 2, 3),),
+        (("az", 1, 3),),
+        (("y", 2, 2, 2), ("az", 0, 3),),
+        (("zz", 2, 4), ("zy", 2, 4), ("y", 2, 3, 1), ("az", 1, 4), ("az", 0, 4),),
+        (("y", 2, 1, 2),),
+        (),
+        (),
+        (("y", 2, 4, 1),),
+        (("y", 2, 3, 2),),
+        (("y", 2, 4, 2),),
+        (),
+    ),
+    (
+        (("bz0", 0), ("bz0", 1), ("by0", 2), ("bz0", 2), ("wo0",), ("by0", 1),),
+        (),
+        (("by0", 0), ("zz", 1, 1), ("zy", 1, 1), ("zz", 0, 1), ("zy", 0, 1),),
+        (("re",),),
+        (("y", 2, 0, 1), ("y", 1, 0, 1),),
+        (("wo1",),),
+        (("zz", 0, 2), ("zy", 0, 2), ("zz", 2, 1), ("zy", 2, 1),),
+        (("zz", 2, 2), ("zy", 2, 2),),
+        (("y", 0, 0, 1),),
+        (("y", 1, 1, 1), ("y", 2, 1, 1),),
+        (("zz", 1, 2), ("zy", 1, 2),),
+        (("y", 2, 0, 2), ("zz", 0, 3), ("zy", 0, 3), ("zz", 0, 4), ("zy", 0, 4), ("y", 0, 1, 1),),
+        (("y", 2, 2, 1), ("y", 1, 2, 1), ("y", 0, 2, 1), ("zz", 1, 3), ("zy", 1, 3), ("zz", 1, 4), ("zy", 1, 4), ("wo2",),),
+        (("y", 0, 3, 1), ("y", 0, 4, 1), ("y", 1, 3, 1), ("y", 1, 0, 2), ("y", 0, 0, 2),),
+        (("y", 0, 1, 2), ("y", 1, 1, 2),),
+        (("y", 1, 4, 1), ("y", 1, 2, 2), ("y", 0, 2, 2),),
+        (("y", 2, 2, 2), ("y", 2, 1, 2), ("zz", 2, 3), ("zy", 2, 3), ("zz", 2, 4), ("zy", 2, 4), ("y", 0, 3, 2), ("y", 1, 3, 2),),
+        (("y", 2, 3, 1), ("y", 0, 4, 2), ("y", 1, 4, 2),),
+        (("y", 2, 4, 1),),
+        (),
+        (("y", 2, 3, 2),),
+        (),
+        (),
+        (("y", 2, 4, 2),),
+        (),
+    ),
+)
 
 
 def dot(a, b):
@@ -141,12 +225,6 @@
     def arrived(ref, sem):
         pltpu.make_async_copy(ref, ref, sem).wait()
 
-    def core0(f):
-        pl.when(c == 0)(f)
-
-    def core1(f):
-        pl.when(c == 1)(f)
-
     partner = dev(cc=1 - c)
     dirc = 1 - 2 * c
     zboth, zlast = hops(NZ)
@@ -252,17 +330,17 @@
 
     def wo_send(r):
         if r in xboth:
-            send(wo.at[(x - r + 1 + NX) % NX, c], wo.at[(x - r + 1 + NX) % NX, c], wo_s.at[2 * r - 1], wo_r.at[2 * r - 1], dev(xx=x + 1))
-            send(wo.at[(x + r - 1) % NX, c], wo.at[(x + r - 1) % NX, c], wo_s.at[2 * r], wo_r.at[2 * r], dev(xx=x - 1))
+            send(wo.at[(x - r + 1 + NX) % NX, c], wo.at[(x - r + 1 + NX) % NX, c], wo_s.at[2 * r - 1], wo_r.at[2 * r - 1], dev(xx=x + 1), False)
+            send(wo.at[(x + r - 1) % NX, c], wo.at[(x + r - 1) % NX, c], wo_s.at[2 * r], wo_r.at[2 * r], dev(xx=x - 1), False)
         elif r == xlast:
             p = (x - dirc * (r - 1) + 2 * NX) % NX
-            send(wo.at[p, c], wo.at[p, c], wo_s.at[NX - 1], wo_r.at[NX - 1], dev(xx=x + dirc))
+            send(wo.at[p, c], wo.at[p, c], wo_s.at[NX - 1], wo_r.at[NX - 1], dev(xx=x + dirc), False)
 
     def wo_wait(r):
         for slot in slots_of(NX, r):
             p = (x + offset_of(NX, slot) + 2 * NX) % NX
             arrived(wo.at[p, c], wo_r.at[slot])
-            send(wo.at[p, c], wo.at[p, c], wop_s.at[slot], wop_r.at[slot], partner)
+            send(wo.at[p, c], wo.at[p, c], wop_s.at[slot], wop_r.at[slot], partner, False)
 
     def zdir(m):
         return dirc * (1 - 2 * (m % 2))
@@ -323,8 +401,7 @@
     RZ = NZ // 2
     RY = NY // 2
 
-    def b_start(m):
-        b1_send(m, 1)
+    def b_first_y(m):
         b2_send(m, 0, 1)
         b_partner(m, 0, 0)
 
@@ -332,6 +409,8 @@
         b1_wait(m, r)
         if r < RZ:
             b1_send(m, r + 1)
+
+    def b_zy(m, r):
         for slot in slots_of(NZ, r):
             b2_send(m, slot, 1)
             b_partner(m, slot, 0)
@@ -357,31 +436,66 @@
         for slot in slots_of(NZ, r):
             a_partner(m, slot)
 
-    def on(core, *steps):
+    def a_first_z(m):
+        a2_send(m, 1)
+        a_partner(m, 0)
+
+    def resid_send():
+        for k in range(1, NX):
+            send(resid.at[x], resid.at[x], re_s.at[k], re_r.at[NX - k], dev(xx=x + k), False)
+
+    def wo_pass(r):
+        wo_wait(r)
+        if r < NX // 2:
+            wo_send(r + 1)
+
+    steps = {
+        "ast": lambda m: a1_send(m, 1),
+        "ay": a_y,
+        "az0": a_first_z,
+        "az": a_z,
+        "bz0": lambda m: b1_send(m, 1),
+        "by0": b_first_y,
+        "zz": b_z,
+        "zy": b_zy,
+        "y": b_y,
+        "wo0": lambda: wo_send(1),
+        "wo1": lambda: wo_pass(1),
+        "wo2": lambda: wo_pass(2),
+        "re": resid_send,
+    }
+
+    def on(core, *todo):
         def run():
-            for f, *a in steps:
-                f(*a)
-
-        if core is None:
-            run()
-        else:
-            pl.when(c == core)(run)
-
-    def both01(f, *a):
-        return [(f, 0, *a), (f, 1, *a)]
+            for f, *a in todo:
+                steps[f](*a)
+
+        pl.when(c == core)(run)
+
+    def gap(name):
+        phase("g_" + name)
+        at = PARTS.index(name)
+        for core in (0, 1):
+            if PLAN[core][at]:
+                on(core, *PLAN[core][at])
 
     phase("send0")
+
+    def q_send(r):
+        if r in yboth:
+            left = 0 if r == 1 else offset_of(NY, 2 * r - 3) % NY
+            right = 0 if r == 1 else offset_of(NY, 2 * r - 2) % NY
+            send(qall.at[left], qall.at[(-r) % NY], q_s.at[2 * r - 1], q_r.at[2 * r - 1], dev(yy=y + 1))
+            send(qall.at[right], qall.at[r], q_s.at[2 * r], q_r.at[2 * r], dev(yy=y - 1))
+        elif r == ylast:
+            member = 0 if r == 1 else (-dirc * (r - 1) + NY) % NY
+            send(qall.at[member], qall.at[r], q_s.at[NY - 1], q_r.at[NY - 1], dev(yy=y + dirc))
+
     kv_send(1)
     kv_partner(0)
-    for k in range(1, NY):
-        send(qall.at[0], qall.at[NY - k], q_s.at[k], q_r.at[NY - k], dev(yy=y + k))
+    q_send(1)
     for d in loc:
         d.wait()
-    on(0, *both01(a1_send, 1))
-    on(1, *both01(b_start))
-    wo_send(1)
-    for k in range(1, NX):
-        send(resid.at[x], resid.at[x], re_s.at[k], re_r.at[NX - k], dev(xx=x + k))
 
     lane = lax.broadcasted_iota(jnp.int32, (T, 256), 1)
     own0 = (lane < 64) | ((lane >= 128) & (lane < 160))
@@ -410,14 +524,22 @@
     mrow[...] = jnp.full_like(mrow, -1e30)
     lrow[...] = jnp.zeros_like(lrow)
     acc[...] = jnp.zeros_like(acc)
+    def q_wait(r):
+        phase(f"qw#r={r}")
+        for slot in slots_of(NY, r):
+            arrived(qall.at[offset_of(NY, slot) % NY], q_r.at[slot])
+        if r < RY:
+            q_send(r + 1)
+        for slot in slots_of(NY, r):
+            spread(offset_of(NY, slot) % NY)
+
+    gap("kvw1")
     kv_wait(1)
-    phase("g1")
-    on(1, *both01(b_z, 1))
-    on(0, *both01(a_y, 1))
-    phase("qwait")
-    for k in range(1, NY):
-        arrived(qall.at[k], q_r.at[k])
-        spread(k)
+    gap("q1")
+    q_wait(1)
+    gap("q2")
+    for r in range(2, RY + 1):
+        q_wait(r)
 
     QB = min(256, NY * T)
     head_rows = ((0, 64), (64, 128), (128, 256))
@@ -458,29 +580,14 @@
         phase(f"att#r={r}")
         attend(ring[0], len(ring))
 
+    gap("att0")
     att(0)
-    kv_wait(2)
-    phase("g2")
-    on(0, *both01(a_y, 2), (a2_send, 0, 1), (a_partner, 0, 0), (a_partner, 1, 0))
-    on(1, *both01(b_y, 0, 1))
-    on(None, (b_start, 2))
-    att(1)
-    kv_wait(3)
-    phase("g3")
-    on(0, (a2_send, 1, 1))
-    on(1, *both01(b_z, 2), *both01(b_y, 0, 2), *both01(b_y, 1, 1))
-    on(None, (b_z, 2, 1))
-    att(2)
-    kv_wait(4)
-    phase("g4")
-    on(0, *both01(a_z, 1))
-    on(1, *both01(b_y, 1, 2), *both01(b_y, 2, 1))
-    on(None, (b_y, 2, 0, 1))
-    att(3)
-    phase("g5")
-    on(1, *both01(b_z, 3))
-    on(None, (b_z, 2, 2), (b_y, 2, 0, 2), (b_y, 2, 1, 1))
-    att(4)
+    for r in range(1, RZ + 1):
+        if r < RZ:
+            gap(f"kvw{r + 1}")
+            kv_wait(r + 1)
+        gap(f"att{r}")
+        att(r)
 
     phase("osend")
     for k in range(NY):
@@ -492,10 +599,7 @@
     for k in range(1, NY):
         send(osend.at[k], orecv.at[NY - k], o_s.at[k], o_r.at[NY - k], dev(yy=y + k))
         send(ssend.at[k], srecv.at[NY - k], st_s.at[k], st_r.at[NY - k], dev(yy=y + k))
-    phase("g6")
-    on(1, *both01(b_y, 2, 2), *both01(b_y, 3, 1))
-    wo_wait(1)
-    wo_send(2)
+    gap("owait")
     phase("owait")
     for k in range(1, NY):
         arrived(orecv.at[k], o_r.at[k])
@@ -518,11 +622,7 @@
     mixed[x] = (heads * ogain_ref[...]).astype(BF16)
     for k in range(1, NX):
         send(mixed.at[x], mixed.at[x], mx_s.at[k], mx_r.at[NX - k], dev(xx=x + k))
-    phase("g7")
-    on(0, *both01(a_z, 2))
-    on(1, *both01(b_z, 4), *both01(b_y, 3, 2))
-    on(None, (b_z, 2, 3), (b_y, 2, 1, 2), (b_y, 2, 2, 1))
-    wo_wait(2)
+    gap("mixw")
     phase("mixw")
     for k in range(1, NX):
         p = (x + k) % NX
@@ -575,22 +675,12 @@
 
         lax.fori_loop(0, len(ring), one, 0)
 
-    phase("widen01")
-    widen(0)
-    widen(1)
-    phase("g8")
-    on(0, *both01(a_z, 3))
-    on(1, *both01(b_y, 4, 1))
-    on(None, (b_z, 2, 4), (b_y, 2, 2, 2), (b_y, 2, 3, 1))
-    phase("widen2")
-    widen(2)
-    phase("g9")
-    on(0, *both01(a_z, 4))
-    on(1, *both01(b_y, 4, 2))
-    phase("widen34")
-    widen(3)
-    widen(4)
-    phase("silu")
+    for r in range(RZ + 1):
+        gap(f"widen{r}")
+        phase(f"widen#r={r}")
+        widen(r)
+    gap("hid")
+    phase("hid")
     g = accg[...]
     hid[...] = (g / (1.0 + jnp.exp(-g)) * accu[...]).astype(BF16)
 
@@ -600,37 +690,27 @@
         part[slot] = s.reshape(NX, R, 256)
         return carry
 
-    def down(first, count):
-        for slot in range(first, first + count):
+    def sums_rows(r):
+        ring = slots_of(NZ, r)
+        return pl.ds(ring[0], len(ring))
+
+    for r in range(RZ + 1):
+        gap(f"down{r}")
+        phase(f"down#r={r}")
+        ring = slots_of(NZ, r)
+        for slot in ring:
             from_partner(2, slot)
-        lax.fori_loop(first, first + count, narrow, 0)
-
-    def sums_send(gr):
-        rows = pl.ds(2 * gr, 2)
+        lax.fori_loop(ring[0], ring[0] + len(ring), narrow, 0)
+        rows = sums_rows(r)
         for k in range(1, NX):
             p = (x + k) % NX
-            send(part.at[rows, p], rsum.at[NX - k, rows], rs_s.at[gr, k], rs_r.at[gr, NX - k], dev(xx=x + k))
-
-    phase("down0")
-    down(0, 4)
-    sums_send(0)
-    sums_send(1)
-    phase("g10")
-    on(None, (b_y, 2, 3, 2), (b_y, 2, 4, 1))
-    phase("down4")
-    down(4, 2)
-    sums_send(2)
-    phase("g11")
-    on(None, (b_y, 2, 4, 2))
-    phase("down6")
-    down(6, 2)
-    sums_send(3)
+            send(part.at[rows, p], rsum.at[NX - k, rows], rs_s.at[r, k], rs_r.at[r, NX - k], dev(xx=x + k))
+    gap("final")
     phase("final")
-    for gr in range(NZ // 2):
-        rows = pl.ds(2 * gr, 2)
+    for r in range(RZ + 1):
         for k in range(1, NX):
-            arrived(rsum.at[k, rows], rs_r.at[gr, k])
-        for slot in (2 * gr, 2 * gr + 1):
+            arrived(rsum.at[k, sums_rows(r)], rs_r.at[r, k])
+        for slot in slots_of(NZ, r):
             p = zpos(slot)
             s = part[slot, x].astype(F32)
             for k in range(1, NX):
@@ -642,6 +722,11 @@
     for d in pend:
         d.wait_send()
 
+    for k in range(1, NX):
+        arrived(wo.at[0, 0], wo_s.at[k])
+        arrived(wo.at[0, 0], wop_s.at[k])
+        arrived(resid.at[0], re_s.at[k])
+
     def sent_a(m):
         arrived(w.at[m, 0, pl.ds(0, NY - 1), 0], w_s1.at[m])
         arrived(w.at[m, pl.ds(0, NZ - 1), :, 0], w_s2.at[m])
@@ -652,9 +737,17 @@
         arrived(w.at[m, :, pl.ds(0, NY - 1), 1], w_s2.at[m])
         arrived(w.at[m, :, :, 1], wp_s.at[m])
 
-    on(0, (sent_a, 0), (sent_a, 1))
-    on(1, (sent_b, 0), (sent_b, 1))
-    on(None, (sent_b, 2))
+    @pl.when(c == 0)
+    def _():
+        sent_a(0)
+        sent_a(1)
+
+    @pl.when(c == 1)
+    def _():
+        sent_b(0)
+        sent_b(1)
+
+    sent_b(2)
 
     phases.close()
 
@@ -743,8 +836,8 @@
             S((NX,)),
             S((NX,)),
             S((NX,)),
-            S((NZ // 2, NX)),
-            S((NZ // 2, NX)),
+            S((NZ // 2 + 1, NX)),
+            S((NZ // 2 + 1, NX)),
             S((3,)),
             S((3,)),
             S((3,)),

time: 93.2 us -> 85.7 us (0.920)
  Pallas kernels: 90.4 us -> 83.2 us
    pallas_call x1, Pallas kernels: 90.4 us -> 83.2 us  [on_device(): pl.pallas_call(functools.partial(kernel, NZ, NX, scales), out_shape=jax.S...]
where the time goes in v3:
time: 85.7 us; the launch traced here: 85.5 us
  Pallas kernels  83.2 us (97%)
  local copies, waits for them, and re-layouts  1.57 us (2%)
    pallas_call x1, Pallas kernels, on_device(): pl.pallas_call(functools.partial(kernel, NZ, NX, scales), out_shape=jax.S...  83.2 us

profile of v3, /device:TPU:1, one launch (start us, length us, event | category | flops | bytes accessed | tf_op | source)
XLA Modules:
  0.0 85.5 jit_solution(8798850968124733079)
XLA Ops:
  0.0 0.7 multiply_sine_fusion
  0.7 83.2 %shard_map.136 = bf16[32,2048]{1,0:T(8,128)(2,1)} custom-call(f32[16,128]{1,0:T(8,128)} %get-tuple-element.6.cos_ref, f32[16,128]{1,0:T(8,128)} %get-tuple-element.5.sin_ref, f32[1,256]{1,0:T(1,128)} %bitcast.13, f32[1,2048]{1,0:T(1,128)} %bitcast.10, f32[1,512]{1,0:T(1,128)} %bitcast.12, bf16[128,512]{1,0:T(8,128)(2,1)} %lat_hbm.1, ...), custom_call_target="tpu_custom_call" | custom-call | tf_op jit(solution)/shard_map/pallas_call | solution.py:787
  83.9 1.6 %copy.16 = bf16[32,2048]{1,0:T(8,128)(2,1)} copy(bf16[32,2048]{1,0:T(8,128)(2,1)} %shard_map.136) | data formatting | bytes 262144
  (2 shorter events, 0.0 us)

commit v4 on v3

--- a/solution.py
+++ b/solution.py
@@ -121,9 +121,9 @@
     scales,
     cos_ref,
     sin_ref,
-    ogain_ref,
-    mgain_ref,
-    lgain_ref,
+    ogain_hbm,
+    mgain_hbm,
+    lgain_hbm,
     lat_hbm,
     kw_hbm,
     vw_hbm,
@@ -136,6 +136,9 @@
     up_hbm,
     down_hbm,
     out_ref,
+    ogain_ref,
+    mgain_ref,
+    lgain_ref,
     lat_ref,
     kw_ref,
     vw_ref,
@@ -163,6 +166,7 @@
     hid,
     part,
     rsum,
+    small_sem,
     loc_sem,
     kv_s,
     kv_r,
@@ -205,8 +209,6 @@
         phases.close()
         phases.enter_context(jax.named_scope(name))
 
-    pend = []
-
     def dev(zz=None, yy=None, cc=None, xx=None):
         zz = z if zz is None else (zz + 2 * NZ) % NZ
         yy = y if yy is None else (yy + 2 * NY) % NY
@@ -214,13 +216,10 @@
         xx = x if xx is None else (xx + 2 * NX) % NX
         return ((zz * NY + yy) * 2 + cc, xx)
 
-    def send(src, dst, ssem, rsem, device, keep=True):
-        d = pltpu.make_async_remote_copy(
+    def send(src, dst, ssem, rsem, device):
+        pltpu.make_async_remote_copy(
             src_ref=src, dst_ref=dst, send_sem=ssem, recv_sem=rsem, device_id=device, device_id_type=MESH
-        )
-        d.start()
-        if keep:
-            pend.append(d)
+        ).start()
 
     def arrived(ref, sem):
         pltpu.make_async_copy(ref, ref, sem).wait()
@@ -239,29 +238,28 @@
     for p in peers:
         pl.semaphore_signal(barrier, inc=1, device_id=p, device_id_type=MESH)
 
-    def local(pairs, first):
-        copies = [
-            pltpu.make_async_copy(a, b, loc_sem.at[first + k]) for k, (a, b) in enumerate(pairs)
-        ]
-        for d in copies:
-            d.start()
-        return copies
-
-    small = local(
-        [(lat_hbm, lat_ref), (kw_hbm, kw_ref), (vw_hbm, vw_ref), (qc_hbm, qc_ref), (qr_hbm, qr_ref), (rk_hbm, rk_ref)],
-        0,
-    )
-    loc = local(
-        [
-            (gate_hbm, w.at[0, z, y, c]),
-            (up_hbm, w.at[1, z, y, c]),
-            (down_hbm, w.at[2, z, y, c]),
-            (ow_hbm, wo.at[x]),
-            (resid_hbm, resid.at[x]),
-        ],
-        6,
-    )
-
+    small = [
+        pltpu.make_async_copy(a, b, small_sem.at[k])
+        for k, (a, b) in enumerate(
+            [(lat_hbm, lat_ref), (lgain_hbm, lgain_ref), (kw_hbm, kw_ref), (vw_hbm, vw_ref), (qc_hbm, qc_ref), (qr_hbm, qr_ref), (rk_hbm, rk_ref)]
+        )
+    ]
+    loc = [
+        pltpu.make_async_copy(a, b, loc_sem.at[k])
+        for k, (a, b) in enumerate(
+            [
+                (gate_hbm, w.at[0, z, y, c]),
+                (up_hbm, w.at[1, z, y, c]),
+                (down_hbm, w.at[2, z, y, c]),
+                (ow_hbm, wo.at[x]),
+                (resid_hbm, resid.at[x]),
+                (ogain_hbm, ogain_ref),
+                (mgain_hbm, mgain_ref),
+            ]
+        )
+    ]
+    for d in small + loc:
+        d.start()
     phase("qkv")
     for d in small:
         d.wait()
@@ -297,10 +295,10 @@
     pl.semaphore_wait(barrier, len(peers))
 
     def kv_copy(src_slot, dst_slot, device):
-        send(kv.at[src_slot, c], kv.at[dst_slot, c], kv_s.at[dst_slot], kv_r.at[dst_slot], device)
+        send(kv.at[src_slot, c], kv.at[dst_slot, c], kv_s, kv_r.at[(dst_slot + 1) // 2], device)
 
     def kv_partner(slot):
-        send(kv.at[slot, c], kv.at[slot, c], kvp_s.at[slot], kvp_r.at[slot], partner)
+        send(kv.at[slot, c], kv.at[slot, c], kvp_s, kvp_r.at[(slot + 1) // 2], partner)
 
     def kv_send(r):
         if r in zboth:
@@ -330,73 +328,70 @@
 
     def wo_send(r):
         if r in xboth:
-            send(wo.at[(x - r + 1 + NX) % NX, c], wo.at[(x - r + 1 + NX) % NX, c], wo_s.at[2 * r - 1], wo_r.at[2 * r - 1], dev(xx=x + 1), False)
-            send(wo.at[(x + r - 1) % NX, c], wo.at[(x + r - 1) % NX, c], wo_s.at[2 * r], wo_r.at[2 * r], dev(xx=x - 1), False)
+            send(wo.at[(x - r + 1 + NX) % NX, c], wo.at[(x - r + 1 + NX) % NX, c], wo_s, wo_r.at[r], dev(xx=x + 1))
+            send(wo.at[(x + r - 1) % NX, c], wo.at[(x + r - 1) % NX, c], wo_s, wo_r.at[r], dev(xx=x - 1))
         elif r == xlast:
             p = (x - dirc * (r - 1) + 2 * NX) % NX
-            send(wo.at[p, c], wo.at[p, c], wo_s.at[NX - 1], wo_r.at[NX - 1], dev(xx=x + dirc), False)
+            send(wo.at[p, c], wo.at[p, c], wo_s, wo_r.at[r], dev(xx=x + dirc))
 
     def wo_wait(r):
+        arrived(wo.at[pl.ds(0, len(slots_of(NX, r))), c], wo_r.at[r])
         for slot in slots_of(NX, r):
             p = (x + offset_of(NX, slot) + 2 * NX) % NX
-            arrived(wo.at[p, c], wo_r.at[slot])
-            send(wo.at[p, c], wo.at[p, c], wop_s.at[slot], wop_r.at[slot], partner, False)
+            send(wo.at[p, c], wo.at[p, c], wop_s, wop_r, partner)
 
     def zdir(m):
         return dirc * (1 - 2 * (m % 2))
 
-    def ring_y(m, zz, cc, r, ssem, rsems):
+    def ring_y(m, zz, cc, r, ssem, rsem):
         if r in yboth:
             a, b = (y - r + 1 + NY) % NY, (y + r - 1) % NY
-            send(w.at[m, zz, a, cc], w.at[m, zz, a, cc], ssem, rsems(2 * r - 1), dev(yy=y + 1), False)
-            send(w.at[m, zz, b, cc], w.at[m, zz, b, cc], ssem, rsems(2 * r), dev(yy=y - 1), False)
+            send(w.at[m, zz, a, cc], w.at[m, zz, a, cc], ssem, rsem, dev(yy=y + 1))
+            send(w.at[m, zz, b, cc], w.at[m, zz, b, cc], ssem, rsem, dev(yy=y - 1))
         elif r == ylast:
             p = (y - zdir(m) * (r - 1) + 2 * NY) % NY
-            send(w.at[m, zz, p, cc], w.at[m, zz, p, cc], ssem, rsems(NY - 1), dev(yy=y + zdir(m)), False)
-
-    def ring_z(m, view, r, ssem, rsems):
+            send(w.at[m, zz, p, cc], w.at[m, zz, p, cc], ssem, rsem, dev(yy=y + zdir(m)))
+
+    def ring_z(m, view, r, ssem, rsem):
         if r in zboth:
             a, b = (z - r + 1 + NZ) % NZ, (z + r - 1) % NZ
-            send(view(a), view(a), ssem, rsems(2 * r - 1), dev(zz=z + 1), False)
-            send(view(b), view(b), ssem, rsems(2 * r), dev(zz=z - 1), False)
+            send(view(a), view(a), ssem, rsem, dev(zz=z + 1))
+            send(view(b), view(b), ssem, rsem, dev(zz=z - 1))
         elif r == zlast:
             p = (z - zdir(m) * (r - 1) + 2 * NZ) % NZ
-            send(view(p), view(p), ssem, rsems(NZ - 1), dev(zz=z + zdir(m)), False)
+            send(view(p), view(p), ssem, rsem, dev(zz=z + zdir(m)))
 
     def a1_send(m, r):
-        ring_y(m, z, 0, r, w_s1.at[m], lambda s: w_r1.at[m, s])
+        ring_y(m, z, 0, r, w_s1.at[m], w_r1.at[m, r])
 
     def a1_wait(m, r):
-        for slot in slots_of(NY, r):
-            arrived(w.at[m, z, ypos(slot), 0], w_r1.at[m, slot])
+        arrived(w.at[m, 0, pl.ds(0, len(slots_of(NY, r))), 0], w_r1.at[m, r])
 
     def a_block(m, zz):
         return w.at[m, zz, :, 0]
 
     def a2_send(m, r):
-        ring_z(m, lambda p: a_block(m, p), r, w_s2.at[m], lambda s: w_r2.at[m, s, 0])
+        ring_z(m, lambda p: a_block(m, p), r, w_s2.at[m], w_r2.at[m, r, 0])
 
     def a_partner(m, slot):
         p = zpos(slot)
-        send(a_block(m, p), a_block(m, p), wp_s.at[m], wp_r.at[m, slot], partner, False)
+        send(a_block(m, p), a_block(m, p), wp_s.at[m], wp_r.at[m, (slot + 1) // 2], partner)
 
     def a2_wait(m, r):
-        for slot in slots_of(NZ, r):
-            arrived(a_block(m, zpos(slot)), w_r2.at[m, slot, 0])
+        arrived(w.at[m, pl.ds(0, len(slots_of(NZ, r))), :, 0], w_r2.at[m, r, 0])
 
     def b1_send(m, r):
-        ring_z(m, lambda p: w.at[m, p, y, c], r, w_s1.at[m], lambda s: w_r1.at[m, s])
+        ring_z(m, lambda p: w.at[m, p, y, c], r, w_s1.at[m], w_r1.at[m, r])
 
     def b1_wait(m, r):
-        for slot in slots_of(NZ, r):
-            arrived(w.at[m, zpos(slot), y, c], w_r1.at[m, slot])
+        arrived(w.at[m, pl.ds(0, len(slots_of(NZ, r))), 0, 0], w_r1.at[m, r])
 
     def b2_send(m, slot, r):
-        ring_y(m, zpos(slot), c, r, w_s2.at[m], lambda s: w_r2.at[m, slot, s])
+        ring_y(m, zpos(slot), c, r, w_s2.at[m], w_r2.at[m, (slot + 1) // 2, r - 1])
 
     def b_partner(m, slot, yslot):
         p = w.at[m, zpos(slot), ypos(yslot), c]
-        send(p, p, wp_s.at[m], wp_r.at[m, slot], partner, False)
+        send(p, p, wp_s.at[m], wp_r.at[m, (slot + 1) // 2], partner)
 
     RZ = NZ // 2
     RY = NY // 2
@@ -416,9 +411,8 @@
             b_partner(m, slot, 0)
 
     def b_y(m, r, k):
+        arrived(w.at[m, pl.ds(0, len(slots_of(NZ, r))), pl.ds(0, len(slots_of(NY, k))), 0], w_r2.at[m, r, k - 1])
         for slot in slots_of(NZ, r):
-            for yslot in slots_of(NY, k):
-                arrived(w.at[m, zpos(slot), ypos(yslot), c], w_r2.at[m, slot, yslot])
             if k < RY:
                 b2_send(m, slot, k + 1)
             for yslot in slots_of(NY, k):
@@ -442,7 +436,7 @@
 
     def resid_send():
         for k in range(1, NX):
-            send(resid.at[x], resid.at[x], re_s.at[k], re_r.at[NX - k], dev(xx=x + k), False)
+            send(resid.at[x], resid.at[x], re_s, re_r, dev(xx=x + k))
 
     def wo_pass(r):
         wo_wait(r)
@@ -485,11 +479,11 @@
         if r in yboth:
             left = 0 if r == 1 else offset_of(NY, 2 * r - 3) % NY
             right = 0 if r == 1 else offset_of(NY, 2 * r - 2) % NY
-            send(qall.at[left], qall.at[(-r) % NY], q_s.at[2 * r - 1], q_r.at[2 * r - 1], dev(yy=y + 1))
-            send(qall.at[right], qall.at[r], q_s.at[2 * r], q_r.at[2 * r], dev(yy=y - 1))
+            send(qall.at[left], qall.at[(-r) % NY], q_s, q_r.at[r], dev(yy=y + 1))
+            send(qall.at[right], qall.at[r], q_s, q_r.at[r], dev(yy=y - 1))
         elif r == ylast:
             member = 0 if r == 1 else (-dirc * (r - 1) + NY) % NY
-            send(qall.at[member], qall.at[r], q_s.at[NY - 1], q_r.at[NY - 1], dev(yy=y + dirc))
+            send(qall.at[member], qall.at[r], q_s, q_r.at[r], dev(yy=y + dirc))
 
     kv_send(1)
     kv_partner(0)
@@ -512,8 +506,8 @@
 
     def kv_wait(r):
         phase(f"kvw#r={r}")
-        for slot in slots_of(NZ, r):
-            arrived(kv.at[slot, c], kv_r.at[slot])
+        ring = slots_of(NZ, r)
+        arrived(kv.at[pl.ds(ring[0], len(ring)), c], kv_r.at[r])
         if r < RZ:
             kv_send(r + 1)
         for slot in slots_of(NZ, r):
@@ -526,8 +520,7 @@
     acc[...] = jnp.zeros_like(acc)
     def q_wait(r):
         phase(f"qw#r={r}")
-        for slot in slots_of(NY, r):
-            arrived(qall.at[offset_of(NY, slot) % NY], q_r.at[slot])
+        arrived(qall.at[pl.ds(0, len(slots_of(NY, r)))], q_r.at[r])
         if r < RY:
             q_send(r + 1)
         for slot in slots_of(NY, r):
@@ -575,8 +568,7 @@
     def att(r):
         phase(f"attw#r={r}")
         ring = slots_of(NZ, r)
-        for slot in ring:
-            arrived(kv.at[slot, 1 - c], kvp_r.at[slot])
+        arrived(kv.at[pl.ds(ring[0], len(ring)), 1 - c], kvp_r.at[r])
         phase(f"att#r={r}")
         attend(ring[0], len(ring))
 
@@ -597,13 +589,12 @@
         ssend[k, 3:6] = lrow[0:3, cols]
         ssend[k, 6:8] = jnp.zeros((2, T), F32)
     for k in range(1, NY):
-        send(osend.at[k], orecv.at[NY - k], o_s.at[k], o_r.at[NY - k], dev(yy=y + k))
-        send(ssend.at[k], srecv.at[NY - k], st_s.at[k], st_r.at[NY - k], dev(yy=y + k))
+        send(osend.at[k], orecv.at[NY - k], o_s, o_r, dev(yy=y + k))
+        send(ssend.at[k], srecv.at[NY - k], st_s, st_r, dev(yy=y + k))
     gap("owait")
     phase("owait")
-    for k in range(1, NY):
-        arrived(orecv.at[k], o_r.at[k])
-        arrived(srecv.at[k], st_r.at[k])
+    arrived(orecv.at[pl.ds(1, NY - 1)], o_r)
+    arrived(srecv.at[pl.ds(1, NY - 1)], st_r)
     phase("merge")
     ms = [ssend[0, 0:3]] + [srecv[k, 0:3] for k in range(1, NY)]
     ls = [ssend[0, 3:6]] + [srecv[k, 3:6] for k in range(1, NY)]
@@ -621,15 +612,12 @@
     heads = jnp.transpose(jnp.concatenate(outs, axis=0))
     mixed[x] = (heads * ogain_ref[...]).astype(BF16)
     for k in range(1, NX):
-        send(mixed.at[x], mixed.at[x], mx_s.at[k], mx_r.at[NX - k], dev(xx=x + k))
+        send(mixed.at[x], mixed.at[x], mx_s, mx_r, dev(xx=x + k))
     gap("mixw")
     phase("mixw")
-    for k in range(1, NX):
-        p = (x + k) % NX
-        arrived(mixed.at[p], mx_r.at[k])
-        arrived(resid.at[p], re_r.at[k])
-    for slot in range(1, NX):
-        arrived(wo.at[(x + offset_of(NX, slot) + 2 * NX) % NX, 1 - c], wop_r.at[slot])
+    arrived(mixed.at[pl.ds(0, NX - 1)], mx_r)
+    arrived(resid.at[pl.ds(0, NX - 1)], re_r)
+    arrived(wo.at[pl.ds(0, NX - 1), 0], wop_r)
     phase("proj")
     mixed_all = jnp.concatenate([mixed[k] for k in range(NX)], axis=1)
 
@@ -652,17 +640,16 @@
     lax.fori_loop(0, D // 256, scale, 0)
 
     phase("mlp0")
-    def from_partner(m, slot):
-        arrived(w.at[m, zpos(slot), :, 1 - c], wp_r.at[m, slot])
+    def from_partner(m, r):
+        arrived(w.at[m, pl.ds(0, len(slots_of(NZ, r))), :, 0], wp_r.at[m, r])
 
     accg[...] = jnp.zeros_like(accg)
     accu[...] = jnp.zeros_like(accu)
     F = accg.shape[1]
 
     def widen(k):
-        for slot in slots_of(NZ, k):
-            from_partner(0, slot)
-            from_partner(1, slot)
+        from_partner(0, k)
+        from_partner(1, k)
         ring = slots_of(NZ, k)
 
         def one(i, carry):
@@ -698,18 +685,16 @@
         gap(f"down{r}")
         phase(f"down#r={r}")
         ring = slots_of(NZ, r)
-        for slot in ring:
-            from_partner(2, slot)
+        from_partner(2, r)
         lax.fori_loop(ring[0], ring[0] + len(ring), narrow, 0)
         rows = sums_rows(r)
         for k in range(1, NX):
             p = (x + k) % NX
-            send(part.at[rows, p], rsum.at[NX - k, rows], rs_s.at[r, k], rs_r.at[r, NX - k], dev(xx=x + k))
+            send(part.at[rows, p], rsum.at[NX - k, rows], rs_s, rs_r.at[r], dev(xx=x + k))
     gap("final")
     phase("final")
     for r in range(RZ + 1):
-        for k in range(1, NX):
-            arrived(rsum.at[k, sums_rows(r)], rs_r.at[r, k])
+        arrived(rsum.at[pl.ds(1, NX - 1), sums_rows(r)], rs_r.at[r])
         for slot in slots_of(NZ, r):
             p = zpos(slot)
             s = part[slot, x].astype(F32)
@@ -719,13 +704,16 @@
             out_ref[:, pl.ds(pl.multiple_of(p * 256, 256), 256)] = s.astype(BF16)
 
     phase("sendw")
-    for d in pend:
-        d.wait_send()
-
-    for k in range(1, NX):
-        arrived(wo.at[0, 0], wo_s.at[k])
-        arrived(wo.at[0, 0], wop_s.at[k])
-        arrived(resid.at[0], re_s.at[k])
+    arrived(kv.at[pl.ds(0, NZ - 1), 0], kv_s)
+    arrived(kv.at[:, 0], kvp_s)
+    arrived(qall.at[pl.ds(0, NY - 1)], q_s)
+    arrived(osend.at[pl.ds(1, NY - 1)], o_s)
+    arrived(ssend.at[pl.ds(1, NY - 1)], st_s)
+    arrived(mixed.at[pl.ds(0, NX - 1)], mx_s)
+    arrived(wo.at[pl.ds(0, NX - 1), 0], wo_s)
+    arrived(wo.at[pl.ds(0, NX - 1), 0], wop_s)
+    arrived(resid.at[pl.ds(0, NX - 1)], re_s)
+    arrived(part.at[:, pl.ds(0, NX - 1)], rs_s)
 
     def sent_a(m):
         arrived(w.at[m, 0, pl.ds(0, NY - 1), 0], w_s1.at[m])
@@ -782,14 +770,22 @@
     vm = pl.BlockSpec(memory_space=pltpu.VMEM)
     hbm = pl.BlockSpec(memory_space=pl.ANY)
     V = pltpu.VMEM
+
+    def pin(a):
+        return pltpu.with_memory_space_constraint(a, pltpu.HBM)
+
     S = pltpu.SemaphoreType.DMA
+    RZ = NZ // 2
     scales = ((64 + ROT_DIM) ** -0.5,) * 2 + ((128 + ROT_DIM) ** -0.5,)
     return pl.pallas_call(
         functools.partial(kernel, NZ, NX, scales),
         out_shape=jax.ShapeDtypeStruct((R, D), BF16),
-        in_specs=[vm] * 5 + [hbm] * 11,
+        in_specs=[vm] * 2 + [hbm] * 14,
         out_specs=vm,
         scratch_shapes=[
+            V((1, output_gain.shape[0]), F32),
+            V((1, D), F32),
+            V((1, key_latent.shape[1]), F32),
             V((T, key_latent.shape[1]), BF16),
             V(key_weight.shape, BF16),
             V(value_weight.shape, BF16),
@@ -817,54 +813,55 @@
             V((T, F), BF16),
             V((NZ, NX, R, 256), BF16),
             V((NX, NZ, R, 256), BF16),
-            S((11,)),
-            S((NZ,)),
-            S((NZ,)),
-            S((NZ,)),
-            S((NZ,)),
-            S((NY,)),
-            S((NY,)),
-            S((NY,)),
-            S((NY,)),
-            S((NY,)),
-            S((NY,)),
-            S((NX,)),
-            S((NX,)),
-            S((NX,)),
-            S((NX,)),
-            S((NX,)),
-            S((NX,)),
-            S((NX,)),
-            S((NX,)),
-            S((NZ // 2 + 1, NX)),
-            S((NZ // 2 + 1, NX)),
+            S((7,)),
+            S((7,)),
+            S(()),
+            S((RZ + 1,)),
+            S(()),
+            S((RZ + 1,)),
+            S(()),
+            S((NY // 2 + 1,)),
+            S(()),
+            S(()),
+            S(()),
+            S(()),
+            S(()),
+            S(()),
+            S(()),
+            S((NX // 2 + 1,)),
+            S(()),
+            S(()),
+            S(()),
+            S(()),
+            S(()),
+            S((RZ + 1,)),
             S((3,)),
             S((3,)),
             S((3,)),
-            S((3, NZ)),
-            S((3, NZ, NY)),
-            S((3, NZ)),
+            S((3, RZ + 1)),
+            S((3, RZ + 1, 2)),
+            S((3, RZ + 1)),
         ],
         compiler_params=pltpu.CompilerParams(
-            collective_id=0, has_side_effects=True, vmem_limit_bytes=60 * 1024 * 1024
+            collective_id=0, has_side_effects=True, vmem_limit_bytes=44 * 1024 * 1024
         ),
     )(
         cos,
         sin,
-        output_gain[None, :],
-        mixer_gain[None, :],
-        latent_gain[None, :],
-        key_latent,
-        key_weight,
-        value_weight,
-        query_content,
-        query_rotary.T,
-        rotary_key.T,
-        residual,
-        output_weight.reshape(2, 128, D),
-        gate_weight,
-        up_weight,
-        down_weight.T,
+        pin(output_gain[None, :]),
+        pin(mixer_gain[None, :]),
+        pin(latent_gain[None, :]),
+        pin(key_latent),
+        pin(key_weight),
+        pin(value_weight),
+        pin(query_content),
+        pin(query_rotary.T),
+        pin(rotary_key.T),
+        pin(residual),
+        pin(output_weight.reshape(2, 128, D)),
+        pin(gate_weight),
+        pin(up_weight),
+        pin(down_weight.T),
     )
 
 

time: 85.7 us -> 82.1 us (0.958)
  Pallas kernels: 83.2 us -> 81.2 us
  local copies, waits for them, and re-layouts: 1.57 us -> 0.66 us
    pallas_call x1, Pallas kernels: 83.2 us -> 81.2 us  [on_device(): pl.pallas_call(functools.partial(kernel, NZ, NX, scales), out_shape=jax.S...]
    unnamed x1, local copies, waits for them, and re-layouts: 1.57 us -> 0.66 us
where the time goes in v4:
time: 82.1 us; the launch traced here: 82 us
  Pallas kernels  81.2 us (99%)
    pallas_call x1, Pallas kernels, on_device(): pl.pallas_call(functools.partial(kernel, NZ, NX, scales), out_shape=jax.S...  81.2 us

profile of v4, /device:TPU:1, one launch (start us, length us, event | category | flops | bytes accessed | tf_op | source)
XLA Modules:
  0.0 82.0 jit_solution(6736146236740136658)
XLA Ops:
  0.0 0.1 multiply_sine_fusion
  0.1 81.2 %shard_map.136 = bf16[32,2048]{1,0:T(8,128)(2,1)S(1)} custom-call(f32[16,128]{1,0:T(8,128)S(1)} %get-tuple-element.6.cos_ref, f32[16,128]{1,0:T(8,128)S(1)} %get-tuple-element.5.sin_ref, f32[1,256]{1,0:T(1,128)} %bitcast.13, f32[1,2048]{1,0:T(1,128)} %bitcast.10, f32[1,512]{1,0:T(1,128)} %bitcast.12, bf16[128,512]{1,0:T(8,128)(2,1)} %lat_hbm.1, ...), custom_call_target="tpu_custom_call" | custom-call | tf_op jit(solution)/shard_map/pallas_call | solution.py:780
  81.3 0.7 copy.16
  (2 shorter events, 0.0 us)

commit v5 on v4

--- a/solution.py
+++ b/solution.py
@@ -17,16 +17,22 @@
 F32 = jnp.float32
 BF16 = jnp.bfloat16
 
+Y_FIRST = ((0, 1, 2), (2,))
+ZDIR = ((1, -1, -1, -1), (-1, 1, 1, -1))
 PARTS = (
     "kvw1",
+    "kvw2",
     "q1",
     "q2",
+    "kvw3",
+    "kx1",
     "att0",
-    "kvw2",
+    "kvw4",
+    "kx2",
     "att1",
-    "kvw3",
+    "kx3",
     "att2",
-    "kvw4",
+    "kx4",
     "att3",
     "att4",
     "owait",
@@ -46,57 +52,65 @@
 )
 PLAN = (
     (
-        (("ast", 0), ("by0", 2), ("ast", 1), ("bz0", 2),),
-        (),
-        (("zz", 2, 1), ("zy", 2, 1),),
-        (("ay", 1, 1),),
-        (("wo0",),),
-        (("y", 2, 1, 1), ("ay", 1, 2),),
-        (),
-        (("y", 2, 0, 1), ("re",), ("az0", 1),),
-        (("ay", 0, 1), ("zz", 2, 2), ("zy", 2, 2),),
-        (("ay", 0, 2), ("az0", 0),),
-        (("wo1",), ("az", 1, 1),),
-        (("az", 0, 1), ("az", 1, 2), ("wo2",),),
-        (("az", 0, 2), ("y", 2, 2, 1),),
-        (),
-        (("y", 2, 0, 2), ("zz", 2, 3), ("zy", 2, 3),),
+        (("ast", 1), ("ast", 0), ("re",),),
+        (("ast", 2), ("by0", 3), ("bz0", 3), ("ay", 1, 1),),
+        (("ay", 0, 1), ("zz", 3, 1),),
+        (("ay", 1, 2), ("az0", 1),),
+        (),
+        (("ay", 0, 2), ("wo0",),),
+        (("az0", 0), ("ay", 2, 1),),
+        (("zz", 3, 2),),
+        (),
+        (("ay", 2, 2), ("az0", 2),),
+        (("zy", 3, 2),),
+        (("az", 0, 1),),
+        (("az", 2, 1),),
+        (),
+        (("az", 1, 1), ("wo1",),),
+        (("y", 3, 0, 1), ("az", 0, 2), ("y", 3, 2, 1), ("az", 2, 2), ("az", 1, 2), ("zz", 3, 3), ("zy", 3, 3),),
+        (("az", 0, 3), ("zy", 3, 1), ("az", 2, 3), ("wo2",),),
         (("az", 1, 3),),
-        (("y", 2, 2, 2), ("az", 0, 3),),
-        (("zz", 2, 4), ("zy", 2, 4), ("y", 2, 3, 1), ("az", 1, 4), ("az", 0, 4),),
-        (("y", 2, 1, 2),),
-        (),
-        (),
-        (("y", 2, 4, 1),),
-        (("y", 2, 3, 2),),
-        (("y", 2, 4, 2),),
+        (("zz", 3, 4), ("zy", 3, 4),),
+        (("y", 3, 1, 1),),
+        (("y", 3, 3, 1),),
+        (("az", 2, 4), ("az", 0, 4), ("az", 1, 4),),
+        (("y", 3, 4, 1),),
+        (("y", 3, 0, 2),),
+        (("y", 3, 1, 2),),
+        (("y", 3, 2, 2),),
+        (("y", 3, 3, 2),),
+        (("y", 3, 4, 2),),
         (),
     ),
     (
-        (("bz0", 0), ("bz0", 1), ("by0", 2), ("bz0", 2), ("wo0",), ("by0", 1),),
-        (),
-        (("by0", 0), ("zz", 1, 1), ("zy", 1, 1), ("zz", 0, 1), ("zy", 0, 1),),
-        (("re",),),
-        (("y", 2, 0, 1), ("y", 1, 0, 1),),
-        (("wo1",),),
-        (("zz", 0, 2), ("zy", 0, 2), ("zz", 2, 1), ("zy", 2, 1),),
-        (("zz", 2, 2), ("zy", 2, 2),),
-        (("y", 0, 0, 1),),
-        (("y", 1, 1, 1), ("y", 2, 1, 1),),
-        (("zz", 1, 2), ("zy", 1, 2),),
-        (("y", 2, 0, 2), ("zz", 0, 3), ("zy", 0, 3), ("zz", 0, 4), ("zy", 0, 4), ("y", 0, 1, 1),),
-        (("y", 2, 2, 1), ("y", 1, 2, 1), ("y", 0, 2, 1), ("zz", 1, 3), ("zy", 1, 3), ("zz", 1, 4), ("zy", 1, 4), ("wo2",),),
-        (("y", 0, 3, 1), ("y", 0, 4, 1), ("y", 1, 3, 1), ("y", 1, 0, 2), ("y", 0, 0, 2),),
-        (("y", 0, 1, 2), ("y", 1, 1, 2),),
-        (("y", 1, 4, 1), ("y", 1, 2, 2), ("y", 0, 2, 2),),
-        (("y", 2, 2, 2), ("y", 2, 1, 2), ("zz", 2, 3), ("zy", 2, 3), ("zz", 2, 4), ("zy", 2, 4), ("y", 0, 3, 2), ("y", 1, 3, 2),),
-        (("y", 2, 3, 1), ("y", 0, 4, 2), ("y", 1, 4, 2),),
-        (("y", 2, 4, 1),),
-        (),
-        (("y", 2, 3, 2),),
-        (),
-        (),
-        (("y", 2, 4, 2),),
+        (("bz0", 1), ("ast", 2), ("bz0", 3), ("re",), ("bz0", 0),),
+        (("zz", 1, 1), ("zz", 3, 1), ("zy", 3, 1), ("zz", 0, 1), ("by0", 3),),
+        (),
+        (("zz", 1, 2), ("zy", 1, 2), ("zz", 0, 2), ("zy", 0, 1), ("zz", 3, 2), ("zy", 3, 2), ("ay", 2, 1),),
+        (("zy", 1, 1),),
+        (("zz", 1, 3), ("zy", 1, 3), ("y", 1, 2, 1),),
+        (("by0", 0), ("zy", 0, 2), ("y", 3, 0, 1), ("by0", 1),),
+        (("zz", 0, 3), ("zz", 0, 4),),
+        (("y", 0, 1, 1), ("ay", 2, 2), ("az0", 2),),
+        (("zz", 1, 4), ("zy", 1, 4),),
+        (("wo0",), ("y", 1, 1, 1),),
+        (("zy", 0, 3), ("y", 0, 0, 1), ("y", 1, 2, 2),),
+        (("az", 2, 1), ("y", 3, 1, 1),),
+        (("y", 1, 3, 1), ("y", 1, 0, 1), ("zy", 0, 4), ("y", 0, 2, 1), ("y", 0, 1, 2), ("y", 1, 4, 1),),
+        (("y", 0, 0, 2), ("y", 0, 3, 1), ("y", 1, 3, 2), ("y", 3, 1, 2), ("wo1",),),
+        (("y", 3, 2, 1), ("az", 2, 2), ("az", 2, 3), ("wo2",), ("y", 0, 4, 1), ("y", 0, 2, 2), ("y", 1, 0, 2),),
+        (("y", 0, 3, 2), ("y", 1, 4, 2), ("y", 1, 1, 2), ("y", 3, 2, 2), ("zz", 3, 3), ("zy", 3, 3), ("zz", 3, 4), ("zy", 3, 4), ("y", 0, 4, 2),),
+        (("y", 3, 0, 2),),
+        (("az", 2, 4), ("y", 3, 3, 1),),
+        (("y", 3, 4, 1),),
+        (),
+        (),
+        (),
+        (),
+        (),
+        (("y", 3, 3, 2),),
+        (("y", 3, 4, 2),),
+        (),
         (),
     ),
 )
@@ -146,7 +160,11 @@
     qr_ref,
     rk_ref,
     w,
-    kv,
+    lats,
+    vwt,
+    k_narrow,
+    k_wide,
+    v_turned,
     qall,
     qx,
     acc,
@@ -172,6 +190,8 @@
     kv_r,
     kvp_s,
     kvp_r,
+    kx_s,
+    kx_r,
     q_s,
     q_r,
     o_s,
@@ -278,13 +298,10 @@
     lat = lat_ref[...].astype(F32)
     lat = lat * lax.rsqrt(jnp.mean(lat * lat, axis=-1, keepdims=True) + EPS)
     lat = (lat * lgain_ref[...]).astype(BF16)
-    keys = dot(lat, kw_ref[...]).astype(BF16)
-    vals = jnp.transpose(dot(lat, vw_ref[...])).astype(BF16)
-    kv[0, c, :, 0:128] = keys[:, 0:128]
-    kv[0, c, :, 128:256] = jnp.transpose(jnp.concatenate(turned(rk_ref, 1) * 4, axis=0)).astype(BF16)
-    kv[0, c, :, 256:384] = keys[:, 128:256]
-    kv[0, c, :, 384:512] = vals[0:128, :]
-    kv[0, c, :, 512:640] = vals[128:256, :]
+    L = lat.shape[1]
+    lats[0, c, :, :, 0:L] = lat.reshape(NX, T // NX, L)
+    rot = jnp.transpose(jnp.concatenate(turned(rk_ref, 1) * 4, axis=0)).astype(BF16)
+    lats[0, c, :, :, L : L + 128] = rot.reshape(NX, T // NX, 128)
 
     turned_q = turned(qr_ref, 3) + [jnp.zeros((ROT_DIM, T), F32)]
     qall[0, :, 0:128] = qc_ref[:, 0:128]
@@ -295,10 +312,10 @@
     pl.semaphore_wait(barrier, len(peers))
 
     def kv_copy(src_slot, dst_slot, device):
-        send(kv.at[src_slot, c], kv.at[dst_slot, c], kv_s, kv_r.at[(dst_slot + 1) // 2], device)
+        send(lats.at[src_slot, c, x], lats.at[dst_slot, c, x], kv_s, kv_r.at[(dst_slot + 1) // 2], device)
 
     def kv_partner(slot):
-        send(kv.at[slot, c], kv.at[slot, c], kvp_s, kvp_r.at[(slot + 1) // 2], partner)
+        send(lats.at[slot, c], lats.at[slot, c], kvp_s, kvp_r.at[(slot + 1) // 2], partner)
 
     def kv_send(r):
         if r in zboth:
@@ -340,58 +357,67 @@
             p = (x + offset_of(NX, slot) + 2 * NX) % NX
             send(wo.at[p, c], wo.at[p, c], wop_s, wop_r, partner)
 
-    def zdir(m):
-        return dirc * (1 - 2 * (m % 2))
-
-    def ring_y(m, zz, cc, r, ssem, rsem):
+    cut = w.shape[5] // 256 * 128
+    units = ((0, 0, w.shape[5]), (1, 0, cut), (1, cut, w.shape[5]), (2, 0, w.shape[5]))
+    core = [0]
+
+    def piece(u, zz, yy, cc):
+        mat, lo, hi = units[u]
+        return w.at[mat, zz, yy, cc, :, lo:hi]
+
+    def some(u, nz, ny):
+        return piece(u, pl.ds(0, nz), pl.ds(0, ny), 0)
+
+    def ring_y(u, zz, r, d, ssem, rsem):
         if r in yboth:
             a, b = (y - r + 1 + NY) % NY, (y + r - 1) % NY
-            send(w.at[m, zz, a, cc], w.at[m, zz, a, cc], ssem, rsem, dev(yy=y + 1))
-            send(w.at[m, zz, b, cc], w.at[m, zz, b, cc], ssem, rsem, dev(yy=y - 1))
+            send(piece(u, zz, a, core[0]), piece(u, zz, a, core[0]), ssem, rsem, dev(yy=y + 1))
+            send(piece(u, zz, b, core[0]), piece(u, zz, b, core[0]), ssem, rsem, dev(yy=y - 1))
         elif r == ylast:
-            p = (y - zdir(m) * (r - 1) + 2 * NY) % NY
-            send(w.at[m, zz, p, cc], w.at[m, zz, p, cc], ssem, rsem, dev(yy=y + zdir(m)))
-
-    def ring_z(m, view, r, ssem, rsem):
+            p = (y - d * (r - 1) + 2 * NY) % NY
+            send(piece(u, zz, p, core[0]), piece(u, zz, p, core[0]), ssem, rsem, dev(yy=y + d))
+
+    def ring_z(u, yy, r, ssem, rsem):
+        d = ZDIR[core[0]][u]
         if r in zboth:
             a, b = (z - r + 1 + NZ) % NZ, (z + r - 1) % NZ
-            send(view(a), view(a), ssem, rsem, dev(zz=z + 1))
-            send(view(b), view(b), ssem, rsem, dev(zz=z - 1))
+            send(piece(u, a, yy, core[0]), piece(u, a, yy, core[0]), ssem, rsem, dev(zz=z + 1))
+            send(piece(u, b, yy, core[0]), piece(u, b, yy, core[0]), ssem, rsem, dev(zz=z - 1))
         elif r == zlast:
-            p = (z - zdir(m) * (r - 1) + 2 * NZ) % NZ
-            send(view(p), view(p), ssem, rsem, dev(zz=z + zdir(m)))
-
-    def a1_send(m, r):
-        ring_y(m, z, 0, r, w_s1.at[m], w_r1.at[m, r])
-
-    def a1_wait(m, r):
-        arrived(w.at[m, 0, pl.ds(0, len(slots_of(NY, r))), 0], w_r1.at[m, r])
-
-    def a_block(m, zz):
-        return w.at[m, zz, :, 0]
-
-    def a2_send(m, r):
-        ring_z(m, lambda p: a_block(m, p), r, w_s2.at[m], w_r2.at[m, r, 0])
-
-    def a_partner(m, slot):
-        p = zpos(slot)
-        send(a_block(m, p), a_block(m, p), wp_s.at[m], wp_r.at[m, (slot + 1) // 2], partner)
-
-    def a2_wait(m, r):
-        arrived(w.at[m, pl.ds(0, len(slots_of(NZ, r))), :, 0], w_r2.at[m, r, 0])
-
-    def b1_send(m, r):
-        ring_z(m, lambda p: w.at[m, p, y, c], r, w_s1.at[m], w_r1.at[m, r])
-
-    def b1_wait(m, r):
-        arrived(w.at[m, pl.ds(0, len(slots_of(NZ, r))), 0, 0], w_r1.at[m, r])
-
-    def b2_send(m, slot, r):
-        ring_y(m, zpos(slot), c, r, w_s2.at[m], w_r2.at[m, (slot + 1) // 2, r - 1])
-
-    def b_partner(m, slot, yslot):
-        p = w.at[m, zpos(slot), ypos(yslot), c]
-        send(p, p, wp_s.at[m], wp_r.at[m, (slot + 1) // 2], partner)
+            p = (z - d * (r - 1) + 2 * NZ) % NZ
+            send(piece(u, p, yy, core[0]), piece(u, p, yy, core[0]), ssem, rsem, dev(zz=z + d))
+
+    every = pl.ds(0, NY)
+
+    def a1_send(u, r):
+        ring_y(u, z, r, ZDIR[core[0]][u], w_s1.at[u], w_r1.at[u, r])
+
+    def a1_wait(u, r):
+        arrived(some(u, 1, len(slots_of(NY, r))), w_r1.at[u, r])
+
+    def a2_send(u, r):
+        ring_z(u, every, r, w_s2.at[u], w_r2.at[u, r, 0])
+
+    def a_partner(u, slot):
+        p = piece(u, zpos(slot), every, core[0])
+        send(p, p, wp_s.at[u], wp_r.at[u, (slot + 1) // 2], partner)
+
+    def a2_wait(u, r):
+        arrived(some(u, len(slots_of(NZ, r)), NY), w_r2.at[u, r, 0])
+
+    def b1_send(u, r):
+        ring_z(u, y, r, w_s1.at[u], w_r1.at[u, r])
+
+    def b1_wait(u, r):
+        arrived(some(u, len(slots_of(NZ, r)), 1), w_r1.at[u, r])
+
+    def b2_send(u, slot, r):
+        d = (1 - 2 * core[0]) * (1 - 2 * (slot % 2))
+        ring_y(u, zpos(slot), r, d, w_s2.at[u], w_r2.at[u, (slot + 1) // 2, r - 1])
+
+    def b_partner(u, slot, yslot):
+        p = piece(u, zpos(slot), ypos(yslot), core[0])
+        send(p, p, wp_s.at[u], wp_r.at[u, (slot + 1) // 2], partner)
 
     RZ = NZ // 2
     RY = NY // 2
@@ -411,7 +437,7 @@
             b_partner(m, slot, 0)
 
     def b_y(m, r, k):
-        arrived(w.at[m, pl.ds(0, len(slots_of(NZ, r))), pl.ds(0, len(slots_of(NY, k))), 0], w_r2.at[m, r, k - 1])
+        arrived(some(m, len(slots_of(NZ, r)), len(slots_of(NY, k))), w_r2.at[m, r, k - 1])
         for slot in slots_of(NZ, r):
             if k < RY:
                 b2_send(m, slot, k + 1)
@@ -459,19 +485,20 @@
         "re": resid_send,
     }
 
-    def on(core, *todo):
+    def on(which, *todo):
         def run():
+            core[0] = which
             for f, *a in todo:
                 steps[f](*a)
 
-        pl.when(c == core)(run)
+        pl.when(c == which)(run)
 
     def gap(name):
         phase("g_" + name)
         at = PARTS.index(name)
-        for core in (0, 1):
-            if PLAN[core][at]:
-                on(core, *PLAN[core][at])
+        for which in (0, 1):
+            if PLAN[which][at]:
+                on(which, *PLAN[which][at])
 
     phase("send0")
 
@@ -507,13 +534,22 @@
     def kv_wait(r):
         phase(f"kvw#r={r}")
         ring = slots_of(NZ, r)
-        arrived(kv.at[pl.ds(ring[0], len(ring)), c], kv_r.at[r])
+        arrived(lats.at[pl.ds(ring[0], len(ring)), c, 0], kv_r.at[r])
         if r < RZ:
             kv_send(r + 1)
-        for slot in slots_of(NZ, r):
+        for slot in ring:
+            for k in range(1, NX):
+                send(lats.at[slot, c, x], lats.at[slot, c, x], kx_s, kx_r.at[r], dev(xx=x + k))
+
+    def kx_wait(r):
+        phase(f"kx#r={r}")
+        ring = slots_of(NZ, r)
+        arrived(lats.at[pl.ds(ring[0], len(ring)), c, pl.ds(0, NX - 1)], kx_r.at[r])
+        for slot in ring:
             kv_partner(slot)
 
     phase("spread0")
+    vwt[...] = jnp.transpose(vw_ref[...].astype(F32)).astype(BF16)
     spread(0)
     mrow[...] = jnp.full_like(mrow, -1e30)
     lrow[...] = jnp.zeros_like(lrow)
@@ -526,33 +562,24 @@
         for slot in slots_of(NY, r):
             spread(offset_of(NY, slot) % NY)
 
-    gap("kvw1")
-    kv_wait(1)
-    gap("q1")
-    q_wait(1)
-    gap("q2")
-    for r in range(2, RY + 1):
-        q_wait(r)
-
     QB = min(256, NY * T)
     head_rows = ((0, 64), (64, 128), (128, 256))
 
     def attend(first, count):
         nk = count * 2 * T
-        k_narrow = kv[first : first + count, :, :, 0:256].reshape(nk, 256)
-        k_wide = kv[first : first + count, :, :, 128:384].reshape(nk, 256)
-
-        def values(h):
-            lo, hi = ((384, 512), (384, 512), (512, 640))[h]
-            r0, r1 = ((0, 64), (64, 128), (0, 128))[h]
-            return jnp.concatenate(
-                [kv[first + s, cc, r0:r1, lo:hi] for s in range(count) for cc in range(2)], axis=1
-            )
+        lat = lats[first : first + count, :, :, :, 0:L].reshape(nk, L)
+        rot = lats[first : first + count, :, :, :, L : L + 128].reshape(nk, 128)
+        keys = dot(lat, kw_ref[...]).astype(BF16)
+        k_narrow[0:nk, 0:128] = keys[:, 0:128]
+        k_narrow[0:nk, 128:256] = rot
+        k_wide[0:nk, 0:128] = rot
+        k_wide[0:nk, 128:256] = keys[:, 128:256]
+        v_turned[:, 0:nk] = dot_nt(vwt[...], lat).astype(BF16)
 
         def block(b, carry):
             cols = pl.ds(pl.multiple_of(b * QB, QB), QB)
             for h in range(3):
-                s = dot_nt(k_narrow if h < 2 else k_wide, qx[h, cols, :]) * (scales[h] * LOG2E)
+                s = dot_nt((k_narrow if h < 2 else k_wide)[0:nk, :], qx[h, cols, :]) * (scales[h] * LOG2E)
                 old = mrow[h : h + 1, cols]
                 new = jnp.maximum(old, jnp.max(s, axis=0, keepdims=True))
                 shrink = jnp.exp2(old - new)
@@ -560,7 +587,7 @@
                 lrow[h : h + 1, cols] = lrow[h : h + 1, cols] * shrink + jnp.sum(p, axis=0, keepdims=True)
                 mrow[h : h + 1, cols] = new
                 r0, r1 = head_rows[h]
-                acc[r0:r1, cols] = acc[r0:r1, cols] * shrink + dot(values(h), p.astype(BF16))
+                acc[r0:r1, cols] = acc[r0:r1, cols] * shrink + dot(v_turned[r0:r1, 0:nk], p.astype(BF16))
             return carry
 
         lax.fori_loop(0, NY * T // QB, block, 0)
@@ -568,18 +595,14 @@
     def att(r):
         phase(f"attw#r={r}")
         ring = slots_of(NZ, r)
-        arrived(kv.at[pl.ds(ring[0], len(ring)), 1 - c], kvp_r.at[r])
+        arrived(lats.at[pl.ds(ring[0], len(ring)), 1 - c], kvp_r.at[r])
         phase(f"att#r={r}")
         attend(ring[0], len(ring))
 
-    gap("att0")
-    att(0)
-    for r in range(1, RZ + 1):
-        if r < RZ:
-            gap(f"kvw{r + 1}")
-            kv_wait(r + 1)
-        gap(f"att{r}")
-        att(r)
+    do = {"kvw": kv_wait, "kx": kx_wait, "q": q_wait, "att": att}
+    for name in PARTS[: PARTS.index("owait")]:
+        gap(name)
+        do[name[:-1]](int(name[-1]))
 
     phase("osend")
     for k in range(NY):
@@ -640,16 +663,16 @@
     lax.fori_loop(0, D // 256, scale, 0)
 
     phase("mlp0")
-    def from_partner(m, r):
-        arrived(w.at[m, pl.ds(0, len(slots_of(NZ, r))), :, 0], wp_r.at[m, r])
+    def from_partner(u, r):
+        arrived(some(u, len(slots_of(NZ, r)), NY), wp_r.at[u, r])
 
     accg[...] = jnp.zeros_like(accg)
     accu[...] = jnp.zeros_like(accu)
     F = accg.shape[1]
 
     def widen(k):
-        from_partner(0, k)
-        from_partner(1, k)
+        for u in range(3):
+            from_partner(u, k)
         ring = slots_of(NZ, k)
 
         def one(i, carry):
@@ -685,7 +708,7 @@
         gap(f"down{r}")
         phase(f"down#r={r}")
         ring = slots_of(NZ, r)
-        from_partner(2, r)
+        from_partner(3, r)
         lax.fori_loop(ring[0], ring[0] + len(ring), narrow, 0)
         rows = sums_rows(r)
         for k in range(1, NX):
@@ -704,8 +727,9 @@
             out_ref[:, pl.ds(pl.multiple_of(p * 256, 256), 256)] = s.astype(BF16)
 
     phase("sendw")
-    arrived(kv.at[pl.ds(0, NZ - 1), 0], kv_s)
-    arrived(kv.at[:, 0], kvp_s)
+    arrived(lats.at[pl.ds(0, NZ - 1), 0, 0], kv_s)
+    arrived(lats.at[:, 0], kvp_s)
+    arrived(lats.at[pl.ds(0, NZ - 1), 0, pl.ds(0, NX - 1)], kx_s)
     arrived(qall.at[pl.ds(0, NY - 1)], q_s)
     arrived(osend.at[pl.ds(1, NY - 1)], o_s)
     arrived(ssend.at[pl.ds(1, NY - 1)], st_s)
@@ -715,27 +739,15 @@
     arrived(resid.at[pl.ds(0, NX - 1)], re_s)
     arrived(part.at[:, pl.ds(0, NX - 1)], rs_s)
 
-    def sent_a(m):
-        arrived(w.at[m, 0, pl.ds(0, NY - 1), 0], w_s1.at[m])
-        arrived(w.at[m, pl.ds(0, NZ - 1), :, 0], w_s2.at[m])
-        arrived(w.at[m, :, :, 0], wp_s.at[m])
-
-    def sent_b(m):
-        arrived(w.at[m, pl.ds(0, NZ - 1), 0, 1], w_s1.at[m])
-        arrived(w.at[m, :, pl.ds(0, NY - 1), 1], w_s2.at[m])
-        arrived(w.at[m, :, :, 1], wp_s.at[m])
-
-    @pl.when(c == 0)
-    def _():
-        sent_a(0)
-        sent_a(1)
-
-    @pl.when(c == 1)
-    def _():
-        sent_b(0)
-        sent_b(1)
-
-    sent_b(2)
+    for which in (0, 1):
+
+        @pl.when(c == which)
+        def _():
+            for u in range(4):
+                first_y = u in Y_FIRST[which]
+                arrived(some(u, 1, NY - 1) if first_y else some(u, NZ - 1, 1), w_s1.at[u])
+                arrived(some(u, NZ - 1, NY) if first_y else some(u, NZ, NY - 1), w_s2.at[u])
+                arrived(some(u, NZ, NY), wp_s.at[u])
 
     phases.close()
 
@@ -793,7 +805,11 @@
             V((query_rotary.shape[1], T), BF16),
             V((ROT_DIM, T), BF16),
             V((3, NZ, NY, 2, R, F), BF16),
-            V((NZ, 2, T, 640), BF16),
+            V((NZ, 2, NX, T // NX, key_latent.shape[1] + 128), BF16),
+            V(value_weight.shape[::-1], BF16),
+            V((4 * T, 256), BF16),
+            V((4 * T, 256), BF16),
+            V((256, 4 * T), BF16),
             V((NY, T, 384), BF16),
             V((3, NY * T, 256), BF16),
             V((256, NY * T), F32),
@@ -820,6 +836,8 @@
             S(()),
             S((RZ + 1,)),
             S(()),
+            S((RZ + 1,)),
+            S(()),
             S((NY // 2 + 1,)),
             S(()),
             S(()),
@@ -835,12 +853,12 @@
             S(()),
             S(()),
             S((RZ + 1,)),
-            S((3,)),
-            S((3,)),
-            S((3,)),
-            S((3, RZ + 1)),
-            S((3, RZ + 1, 2)),
-            S((3, RZ + 1)),
+            S((4,)),
+            S((4,)),
+            S((4,)),
+            S((4, RZ + 1)),
+            S((4, RZ + 1, 2)),
+            S((4, RZ + 1)),
         ],
         compiler_params=pltpu.CompilerParams(
             collective_id=0, has_side_effects=True, vmem_limit_bytes=44 * 1024 * 1024

time: 82.1 us -> 77.3 us (0.942)
  Pallas kernels: 81.2 us -> 76.4 us
    pallas_call x1, Pallas kernels: 81.2 us -> 76.4 us  [on_device(): pl.pallas_call(functools.partial(kernel, NZ, NX, scales), out_shape=jax.S...]
where the time goes in v5:
time: 77.3 us; the launch traced here: 77.2 us
  Pallas kernels  76.4 us (99%)
    pallas_call x1, Pallas kernels, on_device(): pl.pallas_call(functools.partial(kernel, NZ, NX, scales), out_shape=jax.S...  76.4 us

profile of v5, /device:TPU:1, one launch (start us, length us, event | category | flops | bytes accessed | tf_op | source)
XLA Modules:
  0.0 77.2 jit_solution(3987251574149802126)
XLA Ops:
  0.0 0.1 multiply_sine_fusion
  0.1 76.4 %shard_map.136 = bf16[32,2048]{1,0:T(8,128)(2,1)S(1)} custom-call(f32[16,128]{1,0:T(8,128)S(1)} %get-tuple-element.6.cos_ref, f32[16,128]{1,0:T(8,128)S(1)} %get-tuple-element.5.sin_ref, f32[1,256]{1,0:T(1,128)} %bitcast.13, f32[1,2048]{1,0:T(1,128)} %bitcast.10, f32[1,512]{1,0:T(1,128)} %bitcast.12, bf16[128,512]{1,0:T(8,128)(2,1)} %lat_hbm.1, ...), custom_call_target="tpu_custom_call" | custom-call | tf_op jit(solution)/shard_map/pallas_call | solution.py:792
  76.5 0.7 copy.16
  (2 shorter events, 0.0 us)

commit v6 on v5

--- a/solution.py
+++ b/solution.py
@@ -52,59 +52,59 @@
 )
 PLAN = (
     (
-        (("ast", 1), ("ast", 0), ("re",),),
-        (("ast", 2), ("by0", 3), ("bz0", 3), ("ay", 1, 1),),
-        (("ay", 0, 1), ("zz", 3, 1),),
-        (("ay", 1, 2), ("az0", 1),),
-        (),
-        (("ay", 0, 2), ("wo0",),),
-        (("az0", 0), ("ay", 2, 1),),
-        (("zz", 3, 2),),
+        (("ast", 1), ("re",), ("ast", 0), ("bz0", 3),),
+        (("by0", 3), ("ast", 2), ("zz", 3, 1), ("ay", 1, 1),),
+        (("ay", 0, 1), ("ay", 1, 2), ("az0", 1), ("ay", 2, 1),),
+        (),
+        (),
+        (("ay", 0, 2), ("az0", 0),),
+        (("wo0",),),
         (),
         (("ay", 2, 2), ("az0", 2),),
-        (("zy", 3, 2),),
-        (("az", 0, 1),),
+        (("zz", 3, 2), ("zy", 3, 2),),
+        (("y", 3, 0, 1), ("az", 0, 1),),
+        (),
         (("az", 2, 1),),
-        (),
-        (("az", 1, 1), ("wo1",),),
-        (("y", 3, 0, 1), ("az", 0, 2), ("y", 3, 2, 1), ("az", 2, 2), ("az", 1, 2), ("zz", 3, 3), ("zy", 3, 3),),
-        (("az", 0, 3), ("zy", 3, 1), ("az", 2, 3), ("wo2",),),
+        (("wo1",),),
+        (("az", 1, 1),),
+        (("az", 0, 2), ("az", 2, 2), ("az", 1, 2), ("y", 3, 2, 1), ("wo2",),),
+        (("zy", 3, 1), ("zz", 3, 3), ("zy", 3, 3), ("az", 2, 3), ("y", 3, 0, 2), ("az", 0, 3),),
         (("az", 1, 3),),
-        (("zz", 3, 4), ("zy", 3, 4),),
-        (("y", 3, 1, 1),),
+        (("y", 3, 1, 1), ("zz", 3, 4), ("zy", 3, 4),),
         (("y", 3, 3, 1),),
+        (),
         (("az", 2, 4), ("az", 0, 4), ("az", 1, 4),),
-        (("y", 3, 4, 1),),
-        (("y", 3, 0, 2),),
         (("y", 3, 1, 2),),
-        (("y", 3, 2, 2),),
+        (),
+        (("y", 3, 2, 2), ("y", 3, 4, 1),),
+        (),
         (("y", 3, 3, 2),),
         (("y", 3, 4, 2),),
         (),
     ),
     (
-        (("bz0", 1), ("ast", 2), ("bz0", 3), ("re",), ("bz0", 0),),
-        (("zz", 1, 1), ("zz", 3, 1), ("zy", 3, 1), ("zz", 0, 1), ("by0", 3),),
-        (),
-        (("zz", 1, 2), ("zy", 1, 2), ("zz", 0, 2), ("zy", 0, 1), ("zz", 3, 2), ("zy", 3, 2), ("ay", 2, 1),),
-        (("zy", 1, 1),),
-        (("zz", 1, 3), ("zy", 1, 3), ("y", 1, 2, 1),),
-        (("by0", 0), ("zy", 0, 2), ("y", 3, 0, 1), ("by0", 1),),
-        (("zz", 0, 3), ("zz", 0, 4),),
-        (("y", 0, 1, 1), ("ay", 2, 2), ("az0", 2),),
-        (("zz", 1, 4), ("zy", 1, 4),),
-        (("wo0",), ("y", 1, 1, 1),),
-        (("zy", 0, 3), ("y", 0, 0, 1), ("y", 1, 2, 2),),
-        (("az", 2, 1), ("y", 3, 1, 1),),
-        (("y", 1, 3, 1), ("y", 1, 0, 1), ("zy", 0, 4), ("y", 0, 2, 1), ("y", 0, 1, 2), ("y", 1, 4, 1),),
-        (("y", 0, 0, 2), ("y", 0, 3, 1), ("y", 1, 3, 2), ("y", 3, 1, 2), ("wo1",),),
-        (("y", 3, 2, 1), ("az", 2, 2), ("az", 2, 3), ("wo2",), ("y", 0, 4, 1), ("y", 0, 2, 2), ("y", 1, 0, 2),),
-        (("y", 0, 3, 2), ("y", 1, 4, 2), ("y", 1, 1, 2), ("y", 3, 2, 2), ("zz", 3, 3), ("zy", 3, 3), ("zz", 3, 4), ("zy", 3, 4), ("y", 0, 4, 2),),
-        (("y", 3, 0, 2),),
-        (("az", 2, 4), ("y", 3, 3, 1),),
-        (("y", 3, 4, 1),),
-        (),
-        (),
+        (("bz0", 1), ("re",), ("bz0", 3), ("ast", 2), ("bz0", 0),),
+        (("zz", 1, 1), ("zz", 3, 1), ("zy", 3, 1), ("zz", 0, 1),),
+        (),
+        (("by0", 1), ("zz", 3, 2), ("zy", 3, 2), ("zz", 0, 2), ("zy", 0, 2), ("by0", 0), ("zz", 1, 2),),
+        (("ay", 2, 1), ("by0", 3),),
+        (),
+        (("zz", 0, 3), ("zz", 1, 3), ("zy", 1, 3),),
+        (("zy", 1, 1), ("ay", 2, 2), ("az0", 2),),
+        (("y", 0, 0, 1), ("y", 3, 0, 1),),
+        (("zy", 0, 3), ("zz", 1, 4), ("zy", 1, 4),),
+        (("y", 3, 2, 1), ("zy", 1, 2),),
+        (("wo0",), ("zy", 0, 1),),
+        (("y", 1, 1, 1),),
+        (("y", 3, 1, 1), ("zz", 0, 4), ("zy", 0, 4), ("az", 2, 1),),
+        (("y", 1, 2, 1), ("y", 0, 3, 1), ("y", 3, 0, 2),),
+        (("az", 2, 2), ("y", 0, 1, 1), ("wo1",), ("y", 0, 4, 1),),
+        (("y", 1, 3, 1), ("y", 0, 2, 1), ("y", 1, 0, 1), ("wo2",), ("y", 1, 4, 1), ("zz", 3, 3), ("zy", 3, 3), ("az", 2, 3),),
+        (("y", 0, 4, 2), ("y", 0, 1, 2), ("y", 0, 0, 2), ("y", 1, 0, 2),),
+        (("zz", 3, 4), ("zy", 3, 4), ("y", 1, 1, 2),),
+        (("y", 0, 3, 2), ("y", 3, 2, 2), ("y", 3, 1, 2), ("y", 0, 2, 2), ("y", 1, 2, 2),),
+        (("az", 2, 4), ("y", 1, 3, 2),),
+        (("y", 1, 4, 2), ("y", 3, 3, 1), ("y", 3, 4, 1),),
         (),
         (),
         (),
@@ -554,6 +554,8 @@
     mrow[...] = jnp.full_like(mrow, -1e30)
     lrow[...] = jnp.zeros_like(lrow)
     acc[...] = jnp.zeros_like(acc)
+    accg[...] = jnp.zeros_like(accg)
+    accu[...] = jnp.zeros_like(accu)
     def q_wait(r):
         phase(f"qw#r={r}")
         arrived(qall.at[pl.ds(0, len(slots_of(NY, r)))], q_r.at[r])
@@ -590,7 +592,7 @@
                 acc[r0:r1, cols] = acc[r0:r1, cols] * shrink + dot(v_turned[r0:r1, 0:nk], p.astype(BF16))
             return carry
 
-        lax.fori_loop(0, NY * T // QB, block, 0)
+        lax.fori_loop(0, NY * T // QB, block, 0, unroll=True)
 
     def att(r):
         phase(f"attw#r={r}")
@@ -650,24 +652,22 @@
         s = (s + resid[:, :, cols].reshape(T, 256).astype(F32)).astype(BF16)
         mid[n] = s
         s = s.astype(F32)
-        return squares + jnp.sum(s * s, axis=1, keepdims=True)
-
-    squares = lax.fori_loop(0, D // 256, project, jnp.zeros((T, 1), F32))
-    factor = lax.rsqrt(squares / D + EPS)
+        return squares + s * s
+
+    squares = lax.fori_loop(0, D // 256, project, jnp.zeros((T, 256), F32), unroll=4)
+    factor = lax.rsqrt(jnp.sum(squares, axis=1, keepdims=True) / D + EPS)
 
     def scale(n, carry):
         cols = pl.ds(pl.multiple_of(n * 256, 256), 256)
         normed[n] = (mid[n].astype(F32) * factor * mgain_ref[:, cols]).astype(BF16)
         return carry
 
-    lax.fori_loop(0, D // 256, scale, 0)
+    lax.fori_loop(0, D // 256, scale, 0, unroll=4)
 
     phase("mlp0")
     def from_partner(u, r):
         arrived(some(u, len(slots_of(NZ, r)), NY), wp_r.at[u, r])
 
-    accg[...] = jnp.zeros_like(accg)
-    accu[...] = jnp.zeros_like(accu)
     F = accg.shape[1]
 
     def widen(k):
@@ -683,7 +683,7 @@
             accu[...] += dot(n, w[1, p].reshape(256, F))
             return carry
 
-        lax.fori_loop(0, len(ring), one, 0)
+        lax.fori_loop(0, len(ring), one, 0, unroll=True)
 
     for r in range(RZ + 1):
         gap(f"widen{r}")
@@ -709,7 +709,7 @@
         phase(f"down#r={r}")
         ring = slots_of(NZ, r)
         from_partner(3, r)
-        lax.fori_loop(ring[0], ring[0] + len(ring), narrow, 0)
+        lax.fori_loop(ring[0], ring[0] + len(ring), narrow, 0, unroll=True)
         rows = sums_rows(r)
         for k in range(1, NX):
             p = (x + k) % NX

time: 77.3 us -> 77.8 us (level)
  no operation moved by 1% of the time
where the time goes in v6:
time: 77.8 us; the launch traced here: 77.7 us
  Pallas kernels  76.9 us (99%)
    pallas_call x1, Pallas kernels, on_device(): pl.pallas_call(functools.partial(kernel, NZ, NX, scales), out_shape=jax.S...  76.9 us

profile of v6, /device:TPU:1, one launch (start us, length us, event | category | flops | bytes accessed | tf_op | source)
XLA Modules:
  0.0 77.7 jit_solution(5260845986660133595)
XLA Ops:
  0.0 0.1 multiply_sine_fusion
  0.1 76.9 %shard_map.136 = bf16[32,2048]{1,0:T(8,128)(2,1)S(1)} custom-call(f32[16,128]{1,0:T(8,128)S(1)} %get-tuple-element.6.cos_ref, f32[16,128]{1,0:T(8,128)S(1)} %get-tuple-element.5.sin_ref, f32[1,256]{1,0:T(1,128)} %bitcast.13, f32[1,2048]{1,0:T(1,128)} %bitcast.10, f32[1,512]{1,0:T(1,128)} %bitcast.12, bf16[128,512]{1,0:T(8,128)(2,1)} %lat_hbm.1, ...), custom_call_target="tpu_custom_call" | custom-call | tf_op jit(solution)/shard_map/pallas_call | solution.py:792
  77.0 0.7 copy.16
  (2 shorter events, 0.0 us)

commit v7 on v5

--- a/solution.py
+++ b/solution.py
@@ -554,6 +554,8 @@
     mrow[...] = jnp.full_like(mrow, -1e30)
     lrow[...] = jnp.zeros_like(lrow)
     acc[...] = jnp.zeros_like(acc)
+    accg[...] = jnp.zeros_like(accg)
+    accu[...] = jnp.zeros_like(accu)
     def q_wait(r):
         phase(f"qw#r={r}")
         arrived(qall.at[pl.ds(0, len(slots_of(NY, r)))], q_r.at[r])
@@ -590,7 +592,7 @@
                 acc[r0:r1, cols] = acc[r0:r1, cols] * shrink + dot(v_turned[r0:r1, 0:nk], p.astype(BF16))
             return carry
 
-        lax.fori_loop(0, NY * T // QB, block, 0)
+        lax.fori_loop(0, NY * T // QB, block, 0, unroll=True)
 
     def att(r):
         phase(f"attw#r={r}")
@@ -650,24 +652,22 @@
         s = (s + resid[:, :, cols].reshape(T, 256).astype(F32)).astype(BF16)
         mid[n] = s
         s = s.astype(F32)
-        return squares + jnp.sum(s * s, axis=1, keepdims=True)
-
-    squares = lax.fori_loop(0, D // 256, project, jnp.zeros((T, 1), F32))
-    factor = lax.rsqrt(squares / D + EPS)
+        return squares + s * s
+
+    squares = lax.fori_loop(0, D // 256, project, jnp.zeros((T, 256), F32), unroll=4)
+    factor = lax.rsqrt(jnp.sum(squares, axis=1, keepdims=True) / D + EPS)
 
     def scale(n, carry):
         cols = pl.ds(pl.multiple_of(n * 256, 256), 256)
         normed[n] = (mid[n].astype(F32) * factor * mgain_ref[:, cols]).astype(BF16)
         return carry
 
-    lax.fori_loop(0, D // 256, scale, 0)
+    lax.fori_loop(0, D // 256, scale, 0, unroll=4)
 
     phase("mlp0")
     def from_partner(u, r):
         arrived(some(u, len(slots_of(NZ, r)), NY), wp_r.at[u, r])
 
-    accg[...] = jnp.zeros_like(accg)
-    accu[...] = jnp.zeros_like(accu)
     F = accg.shape[1]
 
     def widen(k):
@@ -683,7 +683,7 @@
             accu[...] += dot(n, w[1, p].reshape(256, F))
             return carry
 
-        lax.fori_loop(0, len(ring), one, 0)
+        lax.fori_loop(0, len(ring), one, 0, unroll=True)
 
     for r in range(RZ + 1):
         gap(f"widen{r}")
@@ -709,7 +709,7 @@
         phase(f"down#r={r}")
         ring = slots_of(NZ, r)
         from_partner(3, r)
-        lax.fori_loop(ring[0], ring[0] + len(ring), narrow, 0)
+        lax.fori_loop(ring[0], ring[0] + len(ring), narrow, 0, unroll=True)
         rows = sums_rows(r)
         for k in range(1, NX):
             p = (x + k) % NX

time: 77.3 us -> 76.6 us (level)
  no operation moved by 1% of the time
where the time goes in v7:
time: 76.6 us; the launch traced here: 76.5 us
  Pallas kernels  75.7 us (99%)
    pallas_call x1, Pallas kernels, on_device(): pl.pallas_call(functools.partial(kernel, NZ, NX, scales), out_shape=jax.S...  75.7 us

profile of v7, /device:TPU:1, one launch (start us, length us, event | category | flops | bytes accessed | tf_op | source)
XLA Modules:
  0.0 76.5 jit_solution(14922795630136410849)
XLA Ops:
  0.0 0.1 multiply_sine_fusion
  0.1 75.7 %shard_map.136 = bf16[32,2048]{1,0:T(8,128)(2,1)S(1)} custom-call(f32[16,128]{1,0:T(8,128)S(1)} %get-tuple-element.6.cos_ref, f32[16,128]{1,0:T(8,128)S(1)} %get-tuple-element.5.sin_ref, f32[1,256]{1,0:T(1,128)} %bitcast.13, f32[1,2048]{1,0:T(1,128)} %bitcast.10, f32[1,512]{1,0:T(1,128)} %bitcast.12, bf16[128,512]{1,0:T(8,128)(2,1)} %lat_hbm.1, ...), custom_call_target="tpu_custom_call" | custom-call | tf_op jit(solution)/shard_map/pallas_call | solution.py:792
  75.9 0.7 copy.16
  (2 shorter events, 0.0 us)

commit v8 on v6

--- a/solution.py
+++ b/solution.py
@@ -52,59 +52,59 @@
 )
 PLAN = (
     (
-        (("ast", 1), ("re",), ("ast", 0), ("bz0", 3),),
-        (("by0", 3), ("ast", 2), ("zz", 3, 1), ("ay", 1, 1),),
-        (("ay", 0, 1), ("ay", 1, 2), ("az0", 1), ("ay", 2, 1),),
+        (("bz0", 3), ("re",), ("ast", 1), ("ast", 0), ("ast", 2),),
+        (("by0", 3), ("zz", 3, 1), ("ay", 1, 1),),
+        (("ay", 2, 1),),
+        (("ay", 0, 1), ("ay", 1, 2), ("az0", 1),),
         (),
         (),
         (("ay", 0, 2), ("az0", 0),),
-        (("wo0",),),
-        (),
-        (("ay", 2, 2), ("az0", 2),),
+        (),
+        (),
+        (("wo0",), ("y", 3, 0, 1), ("ay", 2, 2), ("az0", 2), ("az", 1, 1),),
+        (("az", 0, 1),),
+        (),
+        (("zy", 3, 1), ("az", 2, 1),),
+        (),
         (("zz", 3, 2), ("zy", 3, 2),),
-        (("y", 3, 0, 1), ("az", 0, 1),),
-        (),
-        (("az", 2, 1),),
-        (("wo1",),),
-        (("az", 1, 1),),
-        (("az", 0, 2), ("az", 2, 2), ("az", 1, 2), ("y", 3, 2, 1), ("wo2",),),
-        (("zy", 3, 1), ("zz", 3, 3), ("zy", 3, 3), ("az", 2, 3), ("y", 3, 0, 2), ("az", 0, 3),),
-        (("az", 1, 3),),
-        (("y", 3, 1, 1), ("zz", 3, 4), ("zy", 3, 4),),
-        (("y", 3, 3, 1),),
-        (),
+        (("wo1",), ("az", 0, 2), ("az", 2, 2), ("az", 1, 2),),
+        (("y", 3, 2, 1), ("zz", 3, 3), ("zy", 3, 3), ("az", 0, 3), ("y", 3, 1, 1), ("az", 2, 3), ("wo2",),),
+        (("az", 1, 3), ("y", 3, 3, 1),),
+        (("y", 3, 0, 2), ("zz", 3, 4), ("zy", 3, 4),),
+        (("y", 3, 1, 2),),
+        (("y", 3, 2, 2),),
         (("az", 2, 4), ("az", 0, 4), ("az", 1, 4),),
-        (("y", 3, 1, 2),),
-        (),
-        (("y", 3, 2, 2), ("y", 3, 4, 1),),
+        (),
+        (),
+        (("y", 3, 4, 1),),
         (),
         (("y", 3, 3, 2),),
         (("y", 3, 4, 2),),
         (),
     ),
     (
-        (("bz0", 1), ("re",), ("bz0", 3), ("ast", 2), ("bz0", 0),),
+        (("bz0", 1), ("bz0", 3), ("re",), ("ast", 2), ("bz0", 0),),
         (("zz", 1, 1), ("zz", 3, 1), ("zy", 3, 1), ("zz", 0, 1),),
-        (),
-        (("by0", 1), ("zz", 3, 2), ("zy", 3, 2), ("zz", 0, 2), ("zy", 0, 2), ("by0", 0), ("zz", 1, 2),),
-        (("ay", 2, 1), ("by0", 3),),
-        (),
-        (("zz", 0, 3), ("zz", 1, 3), ("zy", 1, 3),),
-        (("zy", 1, 1), ("ay", 2, 2), ("az0", 2),),
-        (("y", 0, 0, 1), ("y", 3, 0, 1),),
-        (("zy", 0, 3), ("zz", 1, 4), ("zy", 1, 4),),
-        (("y", 3, 2, 1), ("zy", 1, 2),),
-        (("wo0",), ("zy", 0, 1),),
-        (("y", 1, 1, 1),),
-        (("y", 3, 1, 1), ("zz", 0, 4), ("zy", 0, 4), ("az", 2, 1),),
-        (("y", 1, 2, 1), ("y", 0, 3, 1), ("y", 3, 0, 2),),
-        (("az", 2, 2), ("y", 0, 1, 1), ("wo1",), ("y", 0, 4, 1),),
-        (("y", 1, 3, 1), ("y", 0, 2, 1), ("y", 1, 0, 1), ("wo2",), ("y", 1, 4, 1), ("zz", 3, 3), ("zy", 3, 3), ("az", 2, 3),),
-        (("y", 0, 4, 2), ("y", 0, 1, 2), ("y", 0, 0, 2), ("y", 1, 0, 2),),
-        (("zz", 3, 4), ("zy", 3, 4), ("y", 1, 1, 2),),
-        (("y", 0, 3, 2), ("y", 3, 2, 2), ("y", 3, 1, 2), ("y", 0, 2, 2), ("y", 1, 2, 2),),
-        (("az", 2, 4), ("y", 1, 3, 2),),
-        (("y", 1, 4, 2), ("y", 3, 3, 1), ("y", 3, 4, 1),),
+        (("ay", 2, 1),),
+        (("zz", 3, 2), ("zy", 3, 2), ("zz", 0, 2), ("zy", 0, 2),),
+        (("zz", 1, 2), ("zy", 1, 2), ("by0", 3),),
+        (("zy", 0, 1),),
+        (("zy", 1, 1),),
+        (("zz", 1, 3), ("zy", 1, 3),),
+        (("ay", 2, 2), ("az0", 2),),
+        (("zz", 0, 3), ("zy", 0, 3),),
+        (("y", 0, 2, 1), ("y", 0, 1, 1),),
+        (("wo0",),),
+        (("by0", 0), ("y", 3, 0, 1), ("zz", 0, 4), ("zy", 0, 4),),
+        (("az", 2, 1), ("y", 0, 2, 2),),
+        (("by0", 1), ("wo1",), ("zz", 1, 4), ("zy", 1, 4), ("az", 2, 2), ("y", 1, 1, 1), ("y", 1, 0, 1), ("y", 1, 3, 1), ("y", 0, 3, 1), ("y", 0, 0, 1), ("y", 0, 4, 1),),
+        (("y", 3, 1, 1), ("y", 1, 4, 1), ("y", 1, 4, 2), ("y", 1, 1, 2), ("az", 2, 3), ("wo2",), ("y", 0, 3, 2),),
+        (("y", 3, 0, 2), ("y", 1, 2, 1), ("y", 0, 0, 2), ("y", 3, 2, 1), ("y", 0, 1, 2), ("y", 1, 3, 2), ("zz", 3, 3), ("zy", 3, 3), ("zz", 3, 4), ("zy", 3, 4), ("y", 1, 2, 2), ("y", 1, 0, 2),),
+        (("az", 2, 4), ("y", 0, 4, 2), ("y", 3, 3, 1),),
+        (("y", 3, 1, 2),),
+        (),
+        (("y", 3, 2, 2), ("y", 3, 4, 1),),
+        (),
         (),
         (),
         (),

time: 77.8 us -> 75.3 us (0.968)
  Pallas kernels: 76.9 us -> 74.4 us
    pallas_call x1, Pallas kernels: 76.9 us -> 74.4 us  [on_device(): pl.pallas_call(functools.partial(kernel, NZ, NX, scales), out_shape=jax.S...]
where the time goes in v8:
time: 75.3 us; the launch traced here: 75.2 us
  Pallas kernels  74.4 us (99%)
    pallas_call x1, Pallas kernels, on_device(): pl.pallas_call(functools.partial(kernel, NZ, NX, scales), out_shape=jax.S...  74.4 us

profile of v8, /device:TPU:1, one launch (start us, length us, event | category | flops | bytes accessed | tf_op | source)
XLA Modules:
  0.0 75.2 jit_solution(14684500253457079034)
XLA Ops:
  0.0 0.1 multiply_sine_fusion
  0.1 74.4 %shard_map.136 = bf16[32,2048]{1,0:T(8,128)(2,1)S(1)} custom-call(f32[16,128]{1,0:T(8,128)S(1)} %get-tuple-element.6.cos_ref, f32[16,128]{1,0:T(8,128)S(1)} %get-tuple-element.5.sin_ref, f32[1,256]{1,0:T(1,128)} %bitcast.13, f32[1,2048]{1,0:T(1,128)} %bitcast.10, f32[1,512]{1,0:T(1,128)} %bitcast.12, bf16[128,512]{1,0:T(8,128)(2,1)} %lat_hbm.1, ...), custom_call_target="tpu_custom_call" | custom-call | tf_op jit(solution)/shard_map/pallas_call | solution.py:792
  74.6 0.7 copy.16
  (2 shorter events, 0.0 us)
